TPU v7x, 256 devices: a whole 4x4x8 slice. The times are simulated.
256 devices in a mesh: ep: 32 (over z, x), tp: 8 (over y, core).
Axes of the slice: x: 4, y: 4, z: 8, core: 2. Of those that a mesh axis runs over, the one named last changes fastest.
Arguments:
- queries: bfloat16 [16384, 1024], P('ep', 'tp'), may hold values from -8 to 8
- keys_values: bfloat16 [16384, 1024], P('ep', 'tp'), may hold values from -60 to 60
- forget_cache: float32 [16, 16384], P('tp'), may hold values from -2460 to 0, as said below
- heads_gain: float32 [1024], replicated, may hold values from 0.1 to 1.9
- output_weight: bfloat16 [1024, 2048], replicated, may hold values from -0.1875 to 0.1875
- expert_tokens: bfloat16 [4096, 2048], P('ep'), may hold values from -600 to 600
- expert_gain: float32 [2048], replicated, may hold values from 0.1 to 1.9
- routes: int32 [4096, 4], P('ep'), may hold values from 0 to 31, all different within a row; in each aligned block of 128 rows (0 to 127, 128 to 255, ...) at most 32 rows name the same one
- route_logits: float32 [4096, 4], P('ep'), may hold values from -6 to 301
- gate_weight: bfloat16 [32, 2048, 2048], P('ep', None, 'tp'), may hold values from -0.5 to 0.5
- up_weight: bfloat16 [32, 2048, 2048], P('ep', None, 'tp'), may hold values from -0.5 to 0.5
- down_weight: bfloat16 [32, 2048, 2048], P('ep', 'tp'), may hold values from -0.015625 to 0.015625
Outputs:
- mixer_out: bfloat16 [16384, 2048], P(('ep', 'tp'))
- moe_out: bfloat16 [4096, 2048], P('ep', 'tp')
Inputs may be any that keep to these rules, and one draw needn't show every extreme that they name: `forget_cache`: each row never rises from one position to the next. `routes`: the 4 experts of a row differ. In each aligned block of 128 rows (one device's tokens) no expert is named more than 32 times, so slot is below 32; some expert is named exactly 32 times in some block.
All inputs are finite; a program needn't handle non-finite values.
Results may differ from a plain program's by a relative error of at most 0.017.
Values may be sent and summed in bfloat16 or wider, within the bound.
A program may use at most 128 MiB of HBM per device.

v0:
```python
import math

import jax
import jax.numpy as jnp
from jax import lax
from jax.sharding import Mesh
from jax.sharding import PartitionSpec as P

HEAD = 64
EP = ("ep_0", "ep_1")
EP_TP = ("ep_0", "ep_1", "tp")


epsilon = 1e-06
clamp_limit = 7.0
sigmoid_slope = 1.702


def gathered_by_axis(array, axes, dim):
    whole = array
    for number in range(len(axes) - 1, -1, -1):
        whole = lax.all_gather(whole, axes[number], axis=dim, tiled=True)
    return whole


def in_blocks(array, dim, devices):
    before, after = (array.shape[:dim], array.shape[dim + 1 :])
    return jnp.moveaxis(array.reshape(*before, devices, -1, *after), dim, 0)


def sent_and_summed(array, axis, dim):
    devices = lax.axis_size(axis)
    parts = lax.all_to_all(in_blocks(array, dim, devices), axis, 0, 0, tiled=True)
    return jnp.sum(parts.astype(jnp.float32), axis=0)


def scaled_rows(values, gain_vector):
    as_float = values.astype(jnp.float32)
    inverse = lax.rsqrt(jnp.mean(as_float * as_float, axis=-1, keepdims=True) + epsilon)
    return (as_float * inverse * gain_vector).astype(jnp.bfloat16)


def assign_slots(routes, experts, capacity):
    row_count, pick_count = routes.shape
    flat_routes = routes.reshape(-1)
    onehot = (flat_routes[:, None] == jnp.arange(experts, dtype=jnp.int32)[None, :]).astype(
        jnp.int32
    )
    earlier = jnp.cumsum(onehot, axis=0) - onehot
    slot_rank = jnp.sum(earlier * onehot, axis=1)
    position = flat_routes * capacity + slot_rank
    owner_row = jnp.arange(row_count * pick_count, dtype=jnp.int32) // pick_count
    slot_token = jnp.full((experts * capacity,), row_count, jnp.int32).at[position].set(owner_row)
    return (position.reshape(row_count, pick_count), slot_token)


def body(
    queries,
    keys_values,
    forget_cache,
    heads_gain,
    output_weight,
    expert_tokens,
    expert_gain,
    routes,
    route_logits,
    gate_weight,
    up_weight,
    down_weight,
):
    row_count = queries.shape[0]
    query_count = queries.shape[1] // HEAD
    key_count = keys_values.shape[1] // (2 * HEAD)
    group_size = query_count // key_count
    offset = lax.axis_index(EP) * row_count
    score_scale = 1.0 / math.sqrt(HEAD)
    count_rows = queries.shape[0]
    segment_positions = offset + jnp.arange(count_rows, dtype=jnp.int32)
    gate_rows = lax.dynamic_slice_in_dim(forget_cache, offset, count_rows, 1)
    segment_bias = gate_rows.T.reshape(count_rows, key_count, group_size, 1)
    segments = [
        (queries.reshape(count_rows, key_count, group_size, HEAD), segment_positions, segment_bias)
    ]
    start_states = tuple(
        [
            (
                jnp.full((grouped.shape[0], key_count, group_size), -jnp.inf, jnp.float32),
                jnp.zeros((grouped.shape[0], key_count, group_size), jnp.float32),
                jnp.zeros((grouped.shape[0], key_count, group_size, HEAD), jnp.float32),
            )
            for grouped, positions, bias in segments
        ]
    )
    piece_rows = gathered_by_axis(keys_values.reshape(row_count, key_count, 2 * HEAD), EP, 0)
    count_rows = piece_rows.shape[0]
    block_width = 512
    blocks = piece_rows.reshape(count_rows // block_width, block_width, key_count, 2 * HEAD)

    def one_block(states, scan_item):
        block_rows, block_index = scan_item
        first_key = block_index * block_width
        key_block = block_rows[:, :, :HEAD]
        value_block = block_rows[:, :, HEAD:]
        key_gate = lax.dynamic_slice_in_dim(forget_cache, first_key, block_width, 1).reshape(
            1, key_count, group_size, block_width
        )
        key_pos = first_key + jnp.arange(block_width, dtype=jnp.int32)
        updated = []
        for (grouped, positions, bias), state in zip(segments, states):

            def take_block(state_in, grouped=grouped, positions=positions, bias=bias):
                running_max, running_sum, weighted = state_in
                scores = (
                    jnp.einsum(
                        "qhgd,khd->qhgk", grouped, key_block, preferred_element_type=jnp.float32
                    )
                    * score_scale
                )
                scores = scores + bias - key_gate
                visible = (key_pos[None, :] <= positions[:, None])[:, None, None, :]
                scores = jnp.where(visible, scores, -jnp.inf)
                new_max = jnp.maximum(running_max, jnp.max(scores, axis=-1))
                safe_max = jnp.where(jnp.isfinite(new_max), new_max, 0.0)
                factor = jnp.exp(running_max - safe_max)
                weights = jnp.exp(scores - safe_max[..., None])
                running_sum = running_sum * factor + jnp.sum(weights, axis=-1)
                weighted = weighted * factor[..., None] + jnp.einsum(
                    "qhgk,khd->qhgd",
                    weights.astype(jnp.bfloat16),
                    value_block,
                    preferred_element_type=jnp.float32,
                )
                return (new_max, running_sum, weighted)

            def keep_state(state_in):
                return state_in

            updated.append(lax.cond(first_key <= positions[-1], take_block, keep_state, state))
        return (tuple(updated), None)

    final_states, _ = lax.scan(
        one_block, start_states, (blocks, jnp.arange(count_rows // block_width, dtype=jnp.int32))
    )
    outputs = [
        (weighted / running_sum[..., None])
        .reshape(running_sum.shape[0], query_count * HEAD)
        .astype(jnp.bfloat16)
        for running_max, running_sum, weighted in final_states
    ]
    attended = outputs[0]
    local_rows = lax.all_to_all(attended, "tp", split_axis=0, concat_axis=1, tiled=True)
    heads_normed = scaled_rows(local_rows, heads_gain)
    mixer_out = jnp.dot(heads_normed, output_weight, preferred_element_type=jnp.float32).astype(
        jnp.bfloat16
    )
    experts_count = lax.axis_size(EP)
    expert_rows, pick_count = routes.shape
    capacity = 2 * expert_rows * pick_count // experts_count
    expert_in = scaled_rows(expert_tokens, expert_gain)
    shifted = route_logits - jnp.max(route_logits, axis=1, keepdims=True)
    raised = jnp.exp(shifted)
    route_weight = raised / jnp.sum(raised, axis=1, keepdims=True)
    position, slot_token = assign_slots(routes, experts_count, capacity)
    model_width = expert_in.shape[1]
    part_width = model_width // lax.axis_size("tp")
    gate_local = gate_weight[0]
    up_local = up_weight[0]
    down_local = down_weight[0]
    own_columns = lax.dynamic_slice_in_dim(
        expert_in, lax.axis_index("tp") * part_width, part_width, 1
    )
    padded = jnp.concatenate([own_columns, jnp.zeros((1, part_width), jnp.bfloat16)], axis=0)
    outgoing = jnp.take(padded, slot_token, axis=0).reshape(experts_count, capacity, part_width)
    arrived = lax.all_to_all(outgoing, EP, split_axis=0, concat_axis=0, tiled=True).reshape(
        experts_count * capacity, part_width
    )
    piece_rows = lax.all_gather(arrived, "tp", axis=1, tiled=True)
    gate_sum = jnp.dot(piece_rows, gate_local, preferred_element_type=jnp.float32)
    up_sum = jnp.dot(piece_rows, up_local, preferred_element_type=jnp.float32)
    gate_cut = jnp.minimum(gate_sum, clamp_limit)
    up_cut = jnp.clip(up_sum, -clamp_limit, clamp_limit)
    hidden = ((up_cut + 1.0) * gate_cut * jax.nn.sigmoid(sigmoid_slope * gate_cut)).astype(
        jnp.bfloat16
    )
    expert_out = sent_and_summed(
        lax.dot_general(
            down_local, hidden, (((0,), (1,)), ((), ())), preferred_element_type=jnp.float32
        ).astype(jnp.bfloat16),
        "tp",
        0,
    ).astype(jnp.bfloat16)
    returned = lax.all_to_all(expert_out, EP, split_axis=1, concat_axis=1, tiled=True)
    picked = jnp.take(returned, position.reshape(-1), axis=1).reshape(
        part_width, expert_rows, pick_count
    )
    moe_out = jnp.einsum("crk,rk->rc", picked.astype(jnp.float32), route_weight).astype(
        jnp.bfloat16
    )
    return (mixer_out, moe_out)


def solution(mesh):
    torus = Mesh(mesh.devices.reshape(8, 4, mesh.shape["tp"]), ("ep_0", "ep_1", "tp"))
    return jax.shard_map(
        body,
        mesh=torus,
        in_specs=(
            P(EP, "tp"),
            P(EP, "tp"),
            P("tp", None),
            P(),
            P(),
            P(EP, None),
            P(),
            P(EP, None),
            P(EP, None),
            P(EP, None, "tp"),
            P(EP, None, "tp"),
            P(EP, "tp", None),
        ),
        out_specs=(P(EP_TP, None), P(EP, "tp")),
        check_vma=False,
    )
```

profile of v0, /device:TPU:2, one launch (start us, length us, event | category | flops | bytes accessed | tf_op | source)
XLA Modules:
  0.0 385.4 jit_solution(9211881118816011675)
XLA Ops:
  7.2 1.2 convert_element_type.73
  8.4 1.2 multiply_reduce_fusion
  9.7 0.8 copy.40
  11.4 1.2 reduce-window.6
  13.2 2.4 scatter_custom_fusion
  15.7 0.8 dynamic-slice
  16.6 3.9 %gather_fusion = bf16[1024,256]{1,0:T(8,128)(2,1)S(1)} fusion(bf16[129,256]{1,0:T(8,128)(2,1)S(1)} %concatenate.3, s32[1024]{0:T(1024)S(1)} %fusion.43), kind=kCustom, calls=%fused_computation | custom fusion | bytes 1052672 | tf_op jit(solution)/shard_map/jit(_take)/gather | solution.py:173
  20.8 28.3 %all_to_all.32 = bf16[32,32,256]{2,1,0:T(8,128)(2,1)} all-to-all(bf16[32,32,256]{2,1,0:T(8,128)(2,1)S(1)} %broadcast_select_fusion), channel_id=1, replica_groups=mesh['ep_0'=8,'ep_1'=4,'tp'=8] {'ep_0','ep_1'}, dimensions={0} | all-to-all | bytes 1048576 | tf_op jit(solution)/shard_map/all_to_all | solution.py:174
  49.2 13.8 %all-gather = bf16[2048,128]{1,0:T(8,128)(2,1)} all-gather(bf16[512,128]{1,0:T(8,128)(2,1)S(1)} %copy-done.1), channel_id=2, replica_groups=mesh['ep_0'=8,'ep_1'=4,'tp'=8] {'ep_1'}, dimensions={0}, use_global_device_ids=true | all-gather | bytes 655360 | tf_op jit(solution)/shard_map/all_gather | solution.py:22
  63.1 21.2 %all-gather.5.cloned.1.call-done = bf16[1024,2048]{1,0:T(8,128)(2,1)} async-done(((bf16[1024,256]{1,0:T(8,128)(2,1)}), bf16[1024,2048]{1,0:T(8,128)(2,1)}) %all-gather.5.cloned.1.call-update) | async-done | bytes 4194320 | tf_op jit(solution)/shard_map/all_gather | solution.py:177
  84.3 4.5 %convolution_minimum_fusion = f32[1024,256]{1,0:T(8,128)} fusion(bf16[1024,2048]{1,0:T(8,128)(2,1)} %all-gather.5.cloned.1.call-done, bf16[1,2048,256]{2,1,0:T(8,128)(2,1)S(1)} %copy-done.6), kind=kOutput, calls=%fused_computation.29 | convolution fusion | flops 1074003968 | bytes 6291456 | tf_op jit(solution)/shard_map/dot_general | solution.py:178
  88.8 8.8 %convolution_convert_fusion = bf16[1024,2048]{1,0:T(8,128)(2,1)} fusion(f32[1024,256]{1,0:T(8,128)} %convolution_minimum_fusion, bf16[1024,2048]{1,0:T(8,128)(2,1)} %all-gather.5.cloned.1.call-done, bf16[1,256,2048]{2,1,0:T(8,128)(2,1)S(1)} %copy-done, bf16[1,2048,256]{2,1,0:T(8,128)(2,1)S(1)} %copy-done.7), kind=kOutput, calls=%fused_computation.27 | convolution fusion | flops 2151940096 | bytes 11534336 | tf_op jit(solution)/shard_map/dot_general | solution.py:186
  97.7 4.6 %copy.58 = bf16[128,8,8,256]{3,2,0,1:T(8,128)(2,1)} copy(bf16[128,8,8,256]{3,2,1,0:T(8,128)(2,1)} %bitcast.128) | data formatting | bytes 8388608 | tf_op jit(solution)/shard_map/reshape | solution.py:28
  102.3 4.7 %all-to-all-start.2 = ((bf16[8,256,1024]{1,2,0:T(8,128)(2,1)}), bf16[8,256,1024]{1,2,0:T(8,128)(2,1)}, u32[]{:S(2)}, u32[]{:S(2)}) async-start(bf16[8,256,1024]{1,2,0:T(8,128)(2,1)} %bitcast.125), calls=%async_computation.2 | async-start | bytes 8388608 | tf_op jit(solution)/shard_map/all_to_all | solution.py:33
  108.0 33.8 %all-gather.7.cloned.1.call-done = bf16[16384,128]{1,0:T(8,128)(2,1)} async-done(((bf16[2048,128]{1,0:T(8,128)(2,1)}), bf16[16384,128]{1,0:T(8,128)(2,1)}) %all-gather.7.cloned.1.call-update) | async-done | bytes 4194320 | tf_op jit(solution)/shard_map/all_gather | solution.py:22
  141.8 6.5 %copy.37 = bf16[32,512,1,128]{1,3,2,0:T(8,128)(2,1)} copy(bf16[32,512,1,128]{3,1,0,2:T(8,128)(2,1)} %bitcast.127) | data formatting | bytes 8388608 | tf_op jit(solution)/shard_map/while | solution.py:141
  148.4 87.1 %while.14 = (s32[]{:T(128)}, f32[512,1,2]{0,2,1:T(2,128)S(1)}, f32[512,1,2]{0,2,1:T(2,128)S(1)}, f32[512,1,2,64]{0,3,2,1:T(8,128)S(1)}, s32[32]{0:T(128)S(1)}, /...) while((s32[]{:T(128)}, f32[512,1,2]{0,2,1:T(2,128)S(1)}, ...), condition=%wide.region_5.6_spmd, body=%wide.region_0.5_spmd.sunk | while | flops 139339264 | bytes 7965025 | solution.py:141
  150.9 3.6 conditional.2
  150.9 0.8 constant_dynamic-slice_fusion
  151.9 0.9 dynamic-slice_bitcast_fusion
  152.8 0.7 fusion.55
  156.9 3.6 conditional.2
  156.9 0.8 constant_dynamic-slice_fusion
  157.9 0.9 dynamic-slice_bitcast_fusion
  235.8 0.8 copy.38
  236.6 4.3 %all-to-all-start = ((bf16[8,64,128]{2,1,0:T(8,128)(2,1)}), bf16[8,64,128]{2,1,0:T(8,128)(2,1)S(1)}, u32[]{:S(2)}, u32[]{:S(2)}) async-start(bf16[8,64,128]{2,1,0:T(8,128)(2,1)} %copy.38), calls=%async_computation | async-start | bytes 262144 | tf_op jit(solution)/shard_map/all_to_all | solution.py:151
  241.1 3.7 reduce_sum.68
  244.8 2.2 all-to-all-done
  247.0 111.8 %all-to-all-start.3 = ((bf16[256,32,32]{0,2,1:T(8,128)(2,1)}), bf16[256,32,32]{0,2,1:T(8,128)(2,1)S(1)}, u32[]{:S(2)}, u32[]{:S(2)}) async-start(bf16[256,32,32]{0,2,1:T(8,128)(2,1)} %bitcast.33), calls=%async_computation.3 | async-start | bytes 1048576 | tf_op jit(solution)/shard_map/all_to_all | solution.py:192
  359.2 3.8 convolution_convert_fusion.1
  363.0 12.5 %all-to-all-done.3 = bf16[256,32,32]{0,2,1:T(8,128)(2,1)S(1)} async-done(((bf16[256,32,32]{0,2,1:T(8,128)(2,1)}), bf16[256,32,32]{0,2,1:T(8,128)(2,1)S(1)}, u32[]{:S(2)}, u32[]{:S(2)}) %all-to-all-start.3) | async-done | bytes 524320 | tf_op jit(solution)/shard_map/all_to_all | solution.py:192
  375.5 1.9 gather_fusion.1
  (206 shorter events, 45.8 us)
Async XLA Ops:
  7.2 81.7 %copy-start = (bf16[1,256,2048]{2,1,0:T(8,128)(2,1)S(1)}, bf16[1,256,2048]{2,1,0:T(8,128)(2,1)}, u32[]{:S(2)}) copy-start(bf16[1,256,2048]{2,1,0:T(8,128)(2,1)} %param.27) | copy-start | bytes 3145732
  7.2 77.1 %all-gather.5.cloned.1.call-start = ((), (), s32[]{:S(2)}) async-start(), calls=%async_computation.4 | async-start | bytes 4718592 | tf_op jit(solution)/shard_map/all_gather | solution.py:177
  10.5 38.8 %copy-start.1 = (bf16[512,128]{1,0:T(8,128)(2,1)S(1)}, bf16[512,128]{1,0:T(8,128)(2,1)}, u32[]{:S(2)}) copy-start(bf16[512,128]{1,0:T(8,128)(2,1)} %param.17) | copy-start | bytes 393220
  16.6 67.7 %copy-start.6 = (bf16[1,2048,256]{2,1,0:T(8,128)(2,1)S(1)}, bf16[1,2048,256]{2,1,0:T(8,128)(2,1)}, u32[]{:S(2)}) copy-start(bf16[1,2048,256]{2,1,0:T(8,128)(2,1)} %param.25) | copy-start | bytes 3145732
  49.2 39.7 %copy-start.7 = (bf16[1,2048,256]{2,1,0:T(8,128)(2,1)S(1)}, bf16[1,2048,256]{2,1,0:T(8,128)(2,1)}, u32[]{:S(2)}) copy-start(bf16[1,2048,256]{2,1,0:T(8,128)(2,1)} %param.26) | copy-start | bytes 3145732
  49.2 92.7 %all-gather.7.cloned.1.call-start = ((), (), s32[]{:S(2)}) async-start(), calls=%async_computation.5 | async-start | bytes 4718592 | tf_op jit(solution)/shard_map/all_gather | solution.py:22
  102.3 4.8 %copy-start.2 = (bf16[512,128]{1,0:T(8,128)(2,1)S(1)}, bf16[512,128]{1,0:T(8,128)(2,1)}, u32[]{:S(2)}) copy-start(bf16[512,128]{1,0:T(8,128)(2,1)} %param.16) | copy-start | bytes 393220
  102.3 134.3 %all-to-all-start.2 = ((bf16[8,256,1024]{1,2,0:T(8,128)(2,1)}), bf16[8,256,1024]{1,2,0:T(8,128)(2,1)}, u32[]{:S(2)}, u32[]{:S(2)}) async-start(bf16[8,256,1024]{1,2,0:T(8,128)(2,1)} %bitcast.125), calls=%async_computation.2 | async-start | bytes 8388608 | tf_op jit(solution)/shard_map/all_to_all | solution.py:33
  148.4 92.5 %copy-start.3 = (s32[128,4]{0,1:T(4,128)S(1)}, s32[128,4]{0,1:T(4,128)}, u32[]{:S(2)}) copy-start(s32[128,4]{0,1:T(4,128)} %param.23) | copy-start | bytes 6148
  148.4 92.7 %copy-start.4 = (f32[128,4]{0,1:T(4,128)S(1)}, f32[128,4]{0,1:T(4,128)}, u32[]{:S(2)}) copy-start(f32[128,4]{0,1:T(4,128)} %param.24) | copy-start | bytes 6148
  235.5 123.6 %copy-start.5 = (f32[1024]{0:T(1024)S(1)}, f32[1024]{0:T(1024)}, u32[]{:S(2)}) copy-start(f32[1024]{0:T(1024)} %param.19) | copy-start | bytes 12292
  236.6 10.4 %all-to-all-start = ((bf16[8,64,128]{2,1,0:T(8,128)(2,1)}), bf16[8,64,128]{2,1,0:T(8,128)(2,1)S(1)}, u32[]{:S(2)}, u32[]{:S(2)}) async-start(bf16[8,64,128]{2,1,0:T(8,128)(2,1)} %copy.38), calls=%async_computation | async-start | bytes 262144 | tf_op jit(solution)/shard_map/all_to_all | solution.py:151
  247.0 128.5 %all-to-all-start.3 = ((bf16[256,32,32]{0,2,1:T(8,128)(2,1)}), bf16[256,32,32]{0,2,1:T(8,128)(2,1)S(1)}, u32[]{:S(2)}, u32[]{:S(2)}) async-start(bf16[256,32,32]{0,2,1:T(8,128)(2,1)} %bitcast.33), calls=%async_computation.3 | async-start | bytes 1048576 | tf_op jit(solution)/shard_map/all_to_all | solution.py:192
Sparse Core Ops, SparseCore 0:
  49.3 34.9 all-gather.4
  86.1 55.6 all-gather.6
where the time goes:
time: 388 us; the launch traced here: 385 us
  starting transfers between devices  121 us (31%)
  waiting for transfers between devices  69.8 us (18%)
  local copies, waits for them, and re-layouts  65.9 us (17%)
  loops' own time  42.4 us (11%)
  blocking collectives  42.2 us (11%)
  matrix products  20 us (5%)
  between operations  14.3 us (4%)
  other arithmetic  9.81 us (3%)
    all_to_all x1, starting transfers between devices, body(): lax.all_to_all(expert_out, EP, split_axis=1, concat_axis=1, tiled=True)  112 us
    another operation x1, loops' own time, body(): lax.scan(one_block, start_states, (blocks, jnp.arange(count_rows // block...  41.9 us
    all_gather x1, waiting for transfers between devices, gathered_by_axis(): whole = lax.all_gather(whole, axes[number], axis=dim, tiled=True)  33.8 us
    all_to_all x1, blocking collectives, body(): lax.all_to_all(outgoing, EP, split_axis=0, concat_axis=0, tiled=True)  28.3 us
    all_gather x1, waiting for transfers between devices, body(): piece_rows = lax.all_gather(arrived, 'tp', axis=1, tiled=True)  21.2 us
    slice x32, local copies, waits for them, and re-layouts, one_block(): positions[-1]  18.9 us
    dynamic_slice x32, local copies, waits for them, and re-layouts, body(): lax.scan(one_block, start_states, (blocks, jnp.arange(count_rows // block...  18.8 us
    all_gather x1, blocking collectives, gathered_by_axis(): whole = lax.all_gather(whole, axes[number], axis=dim, tiled=True)  13.8 us
  transfers between devices with their start and end apart: 5, of which 4 were waited for; matrix products, arithmetic and copies ran while one was open for 21% of the time, Pallas kernels for 0%

commit v1 on v0

--- a/solution.py
+++ b/solution.py
@@ -4,6 +4,8 @@
 import jax.numpy as jnp
 from jax import lax
 from jax.sharding import Mesh
+from jax.experimental import pallas as pl
+from jax.experimental.pallas import tpu as pltpu
 from jax.sharding import PartitionSpec as P
 
 HEAD = 64
@@ -38,6 +40,120 @@
     as_float = values.astype(jnp.float32)
     inverse = lax.rsqrt(jnp.mean(as_float * as_float, axis=-1, keepdims=True) + epsilon)
     return (as_float * inverse * gain_vector).astype(jnp.bfloat16)
+
+
+def split3(x):
+    hi = x.astype(jnp.bfloat16)
+    rest = x - hi.astype(jnp.float32)
+    mid = rest.astype(jnp.bfloat16)
+    low = (rest - mid.astype(jnp.float32)).astype(jnp.bfloat16)
+    return hi, mid, low
+
+
+ROWS = 512
+ASKED = 2 * ROWS
+TILE = 256
+
+
+def query_operand(query_rows, qx):
+    turned = (query_rows.astype(jnp.float32) * (1.0 / math.sqrt(HEAD))).T.astype(jnp.bfloat16)
+    row = lax.broadcasted_iota(jnp.int32, (HEAD, ASKED), 0)
+    col = lax.broadcasted_iota(jnp.int32, (HEAD, ASKED), 1)
+    first = (col < ROWS) & (row < 3)
+    second = (col >= ROWS) & (row >= 3) & (row < 6)
+    qx[0:HEAD, 0:ROWS] = turned[0:HEAD]
+    qx[0:HEAD, ROWS:ASKED] = turned[HEAD : 2 * HEAD]
+    qx[HEAD : 2 * HEAD, :] = jnp.where(first | second, -1.0, 0.0).astype(jnp.bfloat16)
+
+
+def key_operand(block_rows, gate):
+    hi, mid, low = split3(gate)
+    parts = jnp.concatenate(
+        [hi[0:1], mid[0:1], low[0:1], hi[1:2], mid[1:2], low[1:2]], axis=0
+    ).astype(jnp.float32)
+    full = jnp.concatenate(
+        [jnp.zeros((64, ROWS), jnp.float32), parts, jnp.zeros((58, ROWS), jnp.float32)], axis=0
+    )
+    lane = lax.broadcasted_iota(jnp.int32, (ROWS, 2 * HEAD), 1)
+    return jnp.where(lane < HEAD, block_rows, full.T.astype(jnp.bfloat16))
+
+
+def value_operand(block_rows):
+    turned = block_rows.astype(jnp.float32).T[HEAD : 2 * HEAD].astype(jnp.bfloat16)
+    return jnp.concatenate([turned, jnp.ones((16, ROWS), jnp.bfloat16)], axis=0)
+
+
+def attention_kernel(own_ref, q_ref, f_ref, kv_ref, o_ref, qx, top, acc, s_ref):
+    own = own_ref[0]
+    query_operand(q_ref[...], qx)
+    base = pl.multiple_of(own * ROWS, ROWS)
+    start = f_ref[:, pl.ds(base, 128)][:, 0:1]
+    top[...] = jnp.full_like(top, -jnp.inf)
+    acc[...] = jnp.zeros_like(acc)
+
+    def rows_of(block):
+        return pl.ds(pl.multiple_of(block * ROWS, ROWS), ROWS)
+
+    keys = key_operand(kv_ref[rows_of(own), :], f_ref[:, rows_of(own)] - start)
+    for tile in range(ASKED // TILE):
+        cut = slice(tile * TILE, (tile + 1) * TILE)
+        scores = jnp.dot(keys, qx[:, cut], preferred_element_type=jnp.float32)
+        key_at = lax.broadcasted_iota(jnp.int32, (ROWS, TILE), 0)
+        query_at = lax.broadcasted_iota(jnp.int32, (ROWS, TILE), 1) + (tile * TILE) % ROWS
+        s_ref[0, :, cut] = jnp.where(key_at <= query_at, scores, -jnp.inf)
+
+    def take(block, after, slot):
+        keys = key_operand(kv_ref[rows_of(after), :], f_ref[:, rows_of(after)] - start)
+        values = value_operand(kv_ref[rows_of(block), :])
+        for tile in range(ASKED // TILE):
+            cut = slice(tile * TILE, (tile + 1) * TILE)
+            s_ref[1 - slot, :, cut] = jnp.dot(
+                keys, qx[:, cut], preferred_element_type=jnp.float32
+            )
+            scores = s_ref[slot, :, cut]
+            old = top[:, cut]
+            new = jnp.maximum(old, jnp.max(scores, axis=0, keepdims=True))
+            weights = jnp.exp(scores - new).astype(jnp.bfloat16)
+            acc[:, cut] = acc[:, cut] * jnp.exp(old - new) + jnp.dot(
+                values, weights, preferred_element_type=jnp.float32
+            )
+            top[:, cut] = new
+
+    def pair(step, _):
+        first = 2 * step
+        take(jnp.where(first == 0, own, first - 1), jnp.minimum(first, jnp.maximum(own - 1, 0)), 0)
+
+        @pl.when(first + 1 <= own)
+        def _():
+            take(first, jnp.minimum(first + 1, own - 1), 1)
+
+        return 0
+
+    lax.fori_loop(0, (own + 2) // 2, pair, 0)
+    total = acc[...]
+    result = total[0:HEAD] / total[HEAD : HEAD + 1]
+    both = jnp.concatenate([result[:, 0:ROWS], result[:, ROWS:ASKED]], axis=0)
+    o_ref[...] = both.T.astype(jnp.bfloat16)
+
+
+def attention(own, queries, forget, whole):
+    vmem = pl.BlockSpec(memory_space=pltpu.VMEM)
+    return pl.pallas_call(
+        attention_kernel,
+        out_shape=jax.ShapeDtypeStruct((ROWS, 2 * HEAD), jnp.bfloat16),
+        in_specs=[pl.BlockSpec(memory_space=pltpu.SMEM), vmem, vmem, vmem],
+        out_specs=vmem,
+        scratch_shapes=[
+            pltpu.VMEM((2 * HEAD, ASKED), jnp.bfloat16),
+            pltpu.VMEM((1, ASKED), jnp.float32),
+            pltpu.VMEM((HEAD + 16, ASKED), jnp.float32),
+            pltpu.VMEM((2, ROWS, ASKED), jnp.float32),
+        ],
+        compiler_params=pltpu.CompilerParams(vmem_limit_bytes=40 * 2**20),
+        cost_estimate=pl.CostEstimate(
+            flops=10**10, bytes_accessed=5 * 2**20, transcendentals=10**7
+        ),
+    )(own, queries, forget, whole)
 
 
 def assign_slots(routes, experts, capacity):
@@ -68,86 +184,9 @@
     up_weight,
     down_weight,
 ):
-    row_count = queries.shape[0]
-    query_count = queries.shape[1] // HEAD
-    key_count = keys_values.shape[1] // (2 * HEAD)
-    group_size = query_count // key_count
-    offset = lax.axis_index(EP) * row_count
-    score_scale = 1.0 / math.sqrt(HEAD)
-    count_rows = queries.shape[0]
-    segment_positions = offset + jnp.arange(count_rows, dtype=jnp.int32)
-    gate_rows = lax.dynamic_slice_in_dim(forget_cache, offset, count_rows, 1)
-    segment_bias = gate_rows.T.reshape(count_rows, key_count, group_size, 1)
-    segments = [
-        (queries.reshape(count_rows, key_count, group_size, HEAD), segment_positions, segment_bias)
-    ]
-    start_states = tuple(
-        [
-            (
-                jnp.full((grouped.shape[0], key_count, group_size), -jnp.inf, jnp.float32),
-                jnp.zeros((grouped.shape[0], key_count, group_size), jnp.float32),
-                jnp.zeros((grouped.shape[0], key_count, group_size, HEAD), jnp.float32),
-            )
-            for grouped, positions, bias in segments
-        ]
-    )
-    piece_rows = gathered_by_axis(keys_values.reshape(row_count, key_count, 2 * HEAD), EP, 0)
-    count_rows = piece_rows.shape[0]
-    block_width = 512
-    blocks = piece_rows.reshape(count_rows // block_width, block_width, key_count, 2 * HEAD)
-
-    def one_block(states, scan_item):
-        block_rows, block_index = scan_item
-        first_key = block_index * block_width
-        key_block = block_rows[:, :, :HEAD]
-        value_block = block_rows[:, :, HEAD:]
-        key_gate = lax.dynamic_slice_in_dim(forget_cache, first_key, block_width, 1).reshape(
-            1, key_count, group_size, block_width
-        )
-        key_pos = first_key + jnp.arange(block_width, dtype=jnp.int32)
-        updated = []
-        for (grouped, positions, bias), state in zip(segments, states):
-
-            def take_block(state_in, grouped=grouped, positions=positions, bias=bias):
-                running_max, running_sum, weighted = state_in
-                scores = (
-                    jnp.einsum(
-                        "qhgd,khd->qhgk", grouped, key_block, preferred_element_type=jnp.float32
-                    )
-                    * score_scale
-                )
-                scores = scores + bias - key_gate
-                visible = (key_pos[None, :] <= positions[:, None])[:, None, None, :]
-                scores = jnp.where(visible, scores, -jnp.inf)
-                new_max = jnp.maximum(running_max, jnp.max(scores, axis=-1))
-                safe_max = jnp.where(jnp.isfinite(new_max), new_max, 0.0)
-                factor = jnp.exp(running_max - safe_max)
-                weights = jnp.exp(scores - safe_max[..., None])
-                running_sum = running_sum * factor + jnp.sum(weights, axis=-1)
-                weighted = weighted * factor[..., None] + jnp.einsum(
-                    "qhgk,khd->qhgd",
-                    weights.astype(jnp.bfloat16),
-                    value_block,
-                    preferred_element_type=jnp.float32,
-                )
-                return (new_max, running_sum, weighted)
-
-            def keep_state(state_in):
-                return state_in
-
-            updated.append(lax.cond(first_key <= positions[-1], take_block, keep_state, state))
-        return (tuple(updated), None)
-
-    final_states, _ = lax.scan(
-        one_block, start_states, (blocks, jnp.arange(count_rows // block_width, dtype=jnp.int32))
-    )
-    outputs = [
-        (weighted / running_sum[..., None])
-        .reshape(running_sum.shape[0], query_count * HEAD)
-        .astype(jnp.bfloat16)
-        for running_max, running_sum, weighted in final_states
-    ]
-    attended = outputs[0]
+    whole = gathered_by_axis(keys_values, EP, 0)
+    own = lax.axis_index(EP).astype(jnp.int32).reshape(1)
+    attended = attention(own, queries, forget_cache, whole)
     local_rows = lax.all_to_all(attended, "tp", split_axis=0, concat_axis=1, tiled=True)
     heads_normed = scaled_rows(local_rows, heads_gain)
     mixer_out = jnp.dot(heads_normed, output_weight, preferred_element_type=jnp.float32).astype(

time: 388 us -> 210 us (0.54)
  starting transfers between devices: 121 us -> 25.2 us
  local copies, waits for them, and re-layouts: 65.9 us -> 18.6 us
  loops' own time: 42.4 us -> 0 us
  waiting for transfers between devices: 69.8 us -> 80.5 us
    all_to_all x1, starting transfers between devices: 112 us -> 17.1 us  [body(): lax.all_to_all(expert_out, EP, split_axis=1, concat_axis=1, tiled=True)]
    another operation x33 -> x0, loops' own time: 42.4 us -> none  [the longest x1 41.9 us: body(): lax.scan(one_block, start_states, (blocks, jnp.arange(count_rows // block...]
    dynamic_slice x34 -> x0, local copies, waits for them, and re-layouts: 20.3 us -> none  [the longest x32 18.8 us: body(): lax.scan(one_block, start_states, (blocks, jnp.arange(count_rows // block...]
    slice x33 -> x1, local copies, waits for them, and re-layouts: 19.1 us -> 0.22 us  [the longest x32 18.9 us: one_block(): positions[-1]]
    all_to_all x1, waiting for transfers between devices: 0.01 us -> 9.87 us  [sent_and_summed(): lax.all_to_all(in_blocks(array, dim, devices), axis, 0, 0, tiled=True)]
    while x1 -> x0, local copies, waits for them, and re-layouts: 6.49 us -> none  [body(): lax.scan(one_block, start_states, (blocks, jnp.arange(count_rows // block...]
  transfers between devices with their start and end apart: 5 -> 5, of which waited for: 4 -> 5; matrix products, arithmetic and copies ran while one was open for 21% -> 12% of each run, Pallas kernels for 0% -> 1%
where the time goes in v1:
time: 210 us
  waiting for transfers between devices  80.5 us (38%)
  blocking collectives  42.2 us (20%)
  starting transfers between devices  25.2 us (12%)
  local copies, waits for them, and re-layouts  18.6 us (9%)
  matrix products  17.5 us (8%)
  between operations  14.3 us (7%)
  other arithmetic  8.67 us (4%)
  Pallas kernels  2.71 us (1%)
    all_gather x1, waiting for transfers between devices, gathered_by_axis(): whole = lax.all_gather(whole, axes[number], axis=dim, tiled=True)  34.7 us
    all_to_all x1, blocking collectives, body(): lax.all_to_all(outgoing, EP, split_axis=0, concat_axis=0, tiled=True)  28.3 us
    all_gather x1, waiting for transfers between devices, body(): piece_rows = lax.all_gather(arrived, 'tp', axis=1, tiled=True)  21.2 us
    all_to_all x1, starting transfers between devices, body(): lax.all_to_all(expert_out, EP, split_axis=1, concat_axis=1, tiled=True)  17.1 us
    all_gather x1, blocking collectives, gathered_by_axis(): whole = lax.all_gather(whole, axes[number], axis=dim, tiled=True)  13.8 us
    all_to_all x1, waiting for transfers between devices, body(): lax.all_to_all(expert_out, EP, split_axis=1, concat_axis=1, tiled=True)  12.5 us
    all_to_all x1, waiting for transfers between devices, sent_and_summed(): lax.all_to_all(in_blocks(array, dim, devices), axis, 0, 0, tiled=True)  9.87 us
    dot_general x1, matrix products, body(): lax.dot_general(down_local, hidden, (((0,), (1,)), ((), ())), preferred_e...  8.85 us
  transfers between devices with their start and end apart: 5, of which 5 were waited for; matrix products, arithmetic and copies ran while one was open for 12% of the time, Pallas kernels for 1%

profile of v1, /device:TPU:2, one launch (start us, length us, event | category | flops | bytes accessed | tf_op | source)
XLA Modules:
  0.0 209.6 jit_solution(16520922956024138298)
XLA Ops:
  7.2 1.2 convert_element_type.55
  8.5 1.2 multiply_reduce_fusion
  9.7 0.8 copy.27
  10.7 0.7 broadcast_multiply_fusion
  11.4 1.2 reduce-window.6
  12.6 0.2 slice_reduce_fusion
  13.2 2.4 %scatter_custom_fusion = s32[1024]{0:T(1024)S(1)} fusion(s32[512]{0:T(512)S(1)} %bitcast.74, s32[512]{0:T(512)S(1)} %add_select_fusion, s32[]{:T(128)} %constant.84.clone.1), kind=kCustom, calls=%fused_computation.65 | custom fusion | bytes 4100 | tf_op jit(solution)/shard_map/scatter | solution.py:169
  15.8 0.8 dynamic-slice
  16.6 3.9 %gather_fusion = bf16[1024,256]{1,0:T(8,128)(2,1)S(1)} fusion(bf16[129,256]{1,0:T(8,128)(2,1)S(1)} %concatenate.3, s32[1024]{0:T(1024)S(1)} %fusion.33), kind=kCustom, calls=%fused_computation | custom fusion | bytes 1052672 | tf_op jit(solution)/shard_map/jit(_take)/gather | solution.py:212
  20.6 0.2 broadcast_select_fusion
  20.8 28.3 %all_to_all.35 = bf16[32,32,256]{2,1,0:T(8,128)(2,1)} all-to-all(bf16[32,32,256]{2,1,0:T(8,128)(2,1)S(1)} %broadcast_select_fusion), channel_id=1, replica_groups=mesh['ep_0'=8,'ep_1'=4,'tp'=8] {'ep_0','ep_1'}, dimensions={0} | all-to-all | bytes 1048576 | tf_op jit(solution)/shard_map/all_to_all | solution.py:213
  49.2 13.8 %all_gather.9 = bf16[2048,128]{1,0:T(8,128)(2,1)} all-gather(bf16[512,128]{1,0:T(8,128)(2,1)S(1)} %copy-done.4), channel_id=1, replica_groups=mesh['ep_0'=8,'ep_1'=4,'tp'=8] {'ep_1'}, dimensions={0}, use_global_device_ids=true | all-gather | bytes 655360 | tf_op jit(solution)/shard_map/all_gather | solution.py:24
  63.1 21.2 %all-gather.5.cloned.1.call-done = bf16[1024,2048]{1,0:T(8,128)(2,1)} async-done(((bf16[1024,256]{1,0:T(8,128)(2,1)}), bf16[1024,2048]{1,0:T(8,128)(2,1)}) %all-gather.5.cloned.1.call-update) | async-done | bytes 4194320 | tf_op jit(solution)/shard_map/all_gather | solution.py:216
  84.3 4.5 %convolution_minimum_fusion = f32[1024,256]{1,0:T(8,128)} fusion(bf16[1024,2048]{1,0:T(8,128)(2,1)} %all-gather.5.cloned.1.call-done, bf16[1,2048,256]{2,1,0:T(8,128)(2,1)S(1)} %copy-done.8), kind=kOutput, calls=%fused_computation.6 | convolution fusion | flops 1074003968 | bytes 6291456 | tf_op jit(solution)/shard_map/dot_general | solution.py:217
  88.8 8.8 %convolution_convert_fusion = bf16[1024,2048]{1,0:T(8,128)(2,1)} fusion(f32[1024,256]{1,0:T(8,128)} %convolution_minimum_fusion, bf16[1024,2048]{1,0:T(8,128)(2,1)} %all-gather.5.cloned.1.call-done, bf16[1,256,2048]{2,1,0:T(8,128)(2,1)S(1)} %copy-done, bf16[1,2048,256]{2,1,0:T(8,128)(2,1)S(1)} %copy-done.9), kind=kOutput, calls=%fused_computation.4 | convolution fusion | flops 2151940096 | bytes 11534336 | tf_op jit(solution)/shard_map/dot_general | solution.py:225
  97.7 4.6 %copy.44 = bf16[128,8,8,256]{3,2,0,1:T(8,128)(2,1)} copy(bf16[128,8,8,256]{3,2,1,0:T(8,128)(2,1)} %bitcast.68) | data formatting | bytes 8388608 | tf_op jit(solution)/shard_map/reshape | solution.py:30
  102.3 4.7 %all-to-all-start.2 = ((bf16[8,256,1024]{1,2,0:T(8,128)(2,1)}), bf16[8,256,1024]{1,2,0:T(8,128)(2,1)}, u32[]{:S(2)}, u32[]{:S(2)}) async-start(bf16[8,256,1024]{1,2,0:T(8,128)(2,1)} %bitcast.66), calls=%async_computation.2 | async-start | bytes 8388608 | tf_op jit(solution)/shard_map/all_to_all | solution.py:35
  107.2 34.7 %all-gather.3.cloned.1.call-done.kv_ref = bf16[16384,128]{1,0:T(8,128)(2,1)} async-done(((bf16[2048,128]{1,0:T(8,128)(2,1)}), bf16[16384,128]{1,0:T(8,128)(2,1)}) %all-gather.3.cloned.1.call-update) | async-done | bytes 4194320 | tf_op jit(solution)/shard_map/all_gather | solution.py:24
  141.8 2.2 %copy-done.1 = bf16[16384,128]{1,0:T(8,128)(2,1)S(1)} copy-done((bf16[16384,128]{1,0:T(8,128)(2,1)S(1)}, bf16[16384,128]{1,0:T(8,128)(2,1)}, u32[]{:S(2)}) %copy-start.1) | copy-done | bytes 4194328
  144.0 2.7 %shard_map.131 = bf16[512,128]{1,0:T(8,128)(2,1)} custom-call(s32[1]{0:T(128)} %bitcast.own_ref, bf16[512,128]{1,0:T(8,128)(2,1)S(1)} %copy-done.2, f32[2,16384]{1,0:T(2,128)S(1)} %copy-done.3, bf16[16384,128]{1,0:T(8,128)(2,1)S(1)} %copy-done.1), custom_call_target="tpu_custom_call" | custom-call | flops 10000000000 | bytes 5242880 | tf_op jit(solution)/shard_map/pallas_call | solution.py:141
  146.8 9.9 %all-to-all-done.2 = bf16[8,256,1024]{1,2,0:T(8,128)(2,1)} async-done(((bf16[8,256,1024]{1,2,0:T(8,128)(2,1)}), bf16[8,256,1024]{1,2,0:T(8,128)(2,1)}, u32[]{:S(2)}, u32[]{:S(2)}) %all-to-all-start.2) | async-done | bytes 4194336 | tf_op jit(solution)/shard_map/all_to_all | solution.py:35
  156.6 3.4 %all-to-all-start = ((bf16[8,64,128]{2,1,0:T(8,128)(2,1)}), bf16[8,64,128]{2,1,0:T(8,128)(2,1)S(1)}, u32[]{:S(2)}, u32[]{:S(2)}) async-start(bf16[8,64,128]{2,1,0:T(8,128)(2,1)} %bitcast.1), calls=%async_computation | async-start | bytes 262144 | tf_op jit(solution)/shard_map/all_to_all | solution.py:190
  160.0 0.1 copy.31
  160.2 3.7 %reduce_sum.57 = bf16[256,1024]{0,1:T(8,128)(2,1)} reduce(bf16[8,256,1024]{1,2,0:T(8,128)(2,1)} %all-to-all-done.2, bf16[]{:T(256)} %constant.93.clone.1), dimensions={0}, to_apply=%region_6.7 | reduce | flops 1835008 | bytes 4718594 | tf_op jit(solution)/shard_map/reduce_sum | solution.py:36
  163.9 2.1 %all-to-all-done = bf16[8,64,128]{2,1,0:T(8,128)(2,1)S(1)} async-done(((bf16[8,64,128]{2,1,0:T(8,128)(2,1)}), bf16[8,64,128]{2,1,0:T(8,128)(2,1)S(1)}, u32[]{:S(2)}, u32[]{:S(2)}) %all-to-all-start) | async-done | bytes 131104 | tf_op jit(solution)/shard_map/all_to_all | solution.py:190
  166.0 17.1 %all-to-all-start.3 = ((bf16[256,32,32]{0,2,1:T(8,128)(2,1)}), bf16[256,32,32]{0,2,1:T(8,128)(2,1)S(1)}, u32[]{:S(2)}, u32[]{:S(2)}) async-start(bf16[256,32,32]{0,2,1:T(8,128)(2,1)} %bitcast.12), calls=%async_computation.3 | async-start | bytes 1048576 | tf_op jit(solution)/shard_map/all_to_all | solution.py:231
  183.1 0.1 copy.34
  183.4 3.8 %convolution_convert_fusion.1 = bf16[64,2048]{1,0:T(8,128)(2,1)} fusion(bf16[1024,2048]{1,0:T(8,128)(2,1)} %param.16, f32[1024]{0:T(1024)S(1)} %copy-done.7, f32[64]{0:T(128)S(1)} %add_rsqrt_fusion.1, bf16[8,64,128]{2,1,0:T(8,128)(2,1)S(1)} %all-to-all-done), kind=kOutput, calls=%fused_computation.5 | convolution fusion | flops 268828672 | bytes 4591872 | tf_op jit(solution)/shard_map/dot_general | solution.py:192
  187.2 12.5 %all-to-all-done.3 = bf16[256,32,32]{0,2,1:T(8,128)(2,1)S(1)} async-done(((bf16[256,32,32]{0,2,1:T(8,128)(2,1)}), bf16[256,32,32]{0,2,1:T(8,128)(2,1)S(1)}, u32[]{:S(2)}, u32[]{:S(2)}) %all-to-all-start.3) | async-done | bytes 524320 | tf_op jit(solution)/shard_map/all_to_all | solution.py:231
  199.8 1.9 gather_fusion.1
  201.8 0.4 fusion.20
  202.2 0.6 copy.45
  (49 shorter events, 1.4 us)
Async XLA Ops:
  7.2 81.7 %copy-start = (bf16[1,256,2048]{2,1,0:T(8,128)(2,1)S(1)}, bf16[1,256,2048]{2,1,0:T(8,128)(2,1)}, u32[]{:S(2)}) copy-start(bf16[1,256,2048]{2,1,0:T(8,128)(2,1)} %param.23) | copy-start | bytes 3145732
  7.2 77.1 %all-gather.5.cloned.1.call-start = ((), (), s32[]{:S(2)}) async-start(), calls=%async_computation.5 | async-start | bytes 4718592 | tf_op jit(solution)/shard_map/all_gather | solution.py:216
  10.5 38.8 %copy-start.4 = (bf16[512,128]{1,0:T(8,128)(2,1)S(1)}, bf16[512,128]{1,0:T(8,128)(2,1)}, u32[]{:S(2)}) copy-start(bf16[512,128]{1,0:T(8,128)(2,1)} %param.13) | copy-start | bytes 393220
  16.6 67.7 %copy-start.8 = (bf16[1,2048,256]{2,1,0:T(8,128)(2,1)S(1)}, bf16[1,2048,256]{2,1,0:T(8,128)(2,1)}, u32[]{:S(2)}) copy-start(bf16[1,2048,256]{2,1,0:T(8,128)(2,1)} %param.21) | copy-start | bytes 3145732
  49.2 39.7 %copy-start.9 = (bf16[1,2048,256]{2,1,0:T(8,128)(2,1)S(1)}, bf16[1,2048,256]{2,1,0:T(8,128)(2,1)}, u32[]{:S(2)}) copy-start(bf16[1,2048,256]{2,1,0:T(8,128)(2,1)} %param.22) | copy-start | bytes 3145732
  49.2 92.7 %all-gather.3.cloned.1.call-start = ((), (), s32[]{:S(2)}) async-start(), calls=%async_computation.4 | async-start | bytes 4718592 | tf_op jit(solution)/shard_map/all_gather | solution.py:24
  102.3 39.6 %copy-start.2 = (bf16[512,128]{1,0:T(8,128)(2,1)S(1)}, bf16[512,128]{1,0:T(8,128)(2,1)}, u32[]{:S(2)}) copy-start(bf16[512,128]{1,0:T(8,128)(2,1)} %q_ref.1) | copy-start | bytes 393220
  102.3 39.6 %copy-start.3 = (f32[2,16384]{1,0:T(2,128)S(1)}, f32[2,16384]{1,0:T(2,128)}, u32[]{:S(2)}) copy-start(f32[2,16384]{1,0:T(2,128)} %f_ref.1) | copy-start | bytes 393220
  102.3 54.3 %all-to-all-start.2 = ((bf16[8,256,1024]{1,2,0:T(8,128)(2,1)}), bf16[8,256,1024]{1,2,0:T(8,128)(2,1)}, u32[]{:S(2)}, u32[]{:S(2)}) async-start(bf16[8,256,1024]{1,2,0:T(8,128)(2,1)} %bitcast.66), calls=%async_computation.2 | async-start | bytes 8388608 | tf_op jit(solution)/shard_map/all_to_all | solution.py:35
  141.8 2.2 %copy-start.1 = (bf16[16384,128]{1,0:T(8,128)(2,1)S(1)}, bf16[16384,128]{1,0:T(8,128)(2,1)}, u32[]{:S(2)}) copy-start(bf16[16384,128]{1,0:T(8,128)(2,1)} %all-gather.3.cloned.1.call-done.kv_ref) | copy-start | bytes 12582916
  144.0 16.0 %copy-start.5 = (s32[128,4]{0,1:T(4,128)S(1)}, s32[128,4]{0,1:T(4,128)}, u32[]{:S(2)}) copy-start(s32[128,4]{0,1:T(4,128)} %param.19) | copy-start | bytes 6148
  144.0 16.1 %copy-start.6 = (f32[128,4]{0,1:T(4,128)S(1)}, f32[128,4]{0,1:T(4,128)}, u32[]{:S(2)}) copy-start(f32[128,4]{0,1:T(4,128)} %param.20) | copy-start | bytes 6148
  146.8 36.7 %copy-start.7 = (f32[1024]{0:T(1024)S(1)}, f32[1024]{0:T(1024)}, u32[]{:S(2)}) copy-start(f32[1024]{0:T(1024)} %param.15) | copy-start | bytes 12292
  156.6 9.4 %all-to-all-start = ((bf16[8,64,128]{2,1,0:T(8,128)(2,1)}), bf16[8,64,128]{2,1,0:T(8,128)(2,1)S(1)}, u32[]{:S(2)}, u32[]{:S(2)}) async-start(bf16[8,64,128]{2,1,0:T(8,128)(2,1)} %bitcast.1), calls=%async_computation | async-start | bytes 262144 | tf_op jit(solution)/shard_map/all_to_all | solution.py:190
  166.0 33.7 %all-to-all-start.3 = ((bf16[256,32,32]{0,2,1:T(8,128)(2,1)}), bf16[256,32,32]{0,2,1:T(8,128)(2,1)S(1)}, u32[]{:S(2)}, u32[]{:S(2)}) async-start(bf16[256,32,32]{0,2,1:T(8,128)(2,1)} %bitcast.12), calls=%async_computation.3 | async-start | bytes 1048576 | tf_op jit(solution)/shard_map/all_to_all | solution.py:231
Sparse Core Ops, SparseCore 0:
  49.3 34.9 all-gather.4
  86.1 55.6 all-gather.2

commit v2 on v1

--- a/solution.py
+++ b/solution.py
@@ -23,17 +23,6 @@
     for number in range(len(axes) - 1, -1, -1):
         whole = lax.all_gather(whole, axes[number], axis=dim, tiled=True)
     return whole
-
-
-def in_blocks(array, dim, devices):
-    before, after = (array.shape[:dim], array.shape[dim + 1 :])
-    return jnp.moveaxis(array.reshape(*before, devices, -1, *after), dim, 0)
-
-
-def sent_and_summed(array, axis, dim):
-    devices = lax.axis_size(axis)
-    parts = lax.all_to_all(in_blocks(array, dim, devices), axis, 0, 0, tiled=True)
-    return jnp.sum(parts.astype(jnp.float32), axis=0)
 
 
 def scaled_rows(values, gain_vector):
@@ -83,7 +72,7 @@
     return jnp.concatenate([turned, jnp.ones((16, ROWS), jnp.bfloat16)], axis=0)
 
 
-def attention_kernel(own_ref, q_ref, f_ref, kv_ref, o_ref, qx, top, acc, s_ref):
+def attention_kernel(own_ref, q_ref, f_ref, kv_ref, later_ref, o_ref, qx, top, acc, s_ref):
     own = own_ref[0]
     query_operand(q_ref[...], qx)
     base = pl.multiple_of(own * ROWS, ROWS)
@@ -136,12 +125,18 @@
     o_ref[...] = both.T.astype(jnp.bfloat16)
 
 
-def attention(own, queries, forget, whole):
+def attention(own, queries, forget, whole, later):
     vmem = pl.BlockSpec(memory_space=pltpu.VMEM)
     return pl.pallas_call(
         attention_kernel,
         out_shape=jax.ShapeDtypeStruct((ROWS, 2 * HEAD), jnp.bfloat16),
-        in_specs=[pl.BlockSpec(memory_space=pltpu.SMEM), vmem, vmem, vmem],
+        in_specs=[
+            pl.BlockSpec(memory_space=pltpu.SMEM),
+            vmem,
+            vmem,
+            vmem,
+            pl.BlockSpec(memory_space=pl.ANY),
+        ],
         out_specs=vmem,
         scratch_shapes=[
             pltpu.VMEM((2 * HEAD, ASKED), jnp.bfloat16),
@@ -153,21 +148,348 @@
         cost_estimate=pl.CostEstimate(
             flops=10**10, bytes_accessed=5 * 2**20, transcendentals=10**7
         ),
-    )(own, queries, forget, whole)
-
-
-def assign_slots(routes, experts, capacity):
-    row_count, pick_count = routes.shape
-    flat_routes = routes.reshape(-1)
-    onehot = (flat_routes[:, None] == jnp.arange(experts, dtype=jnp.int32)[None, :]).astype(
-        jnp.int32
-    )
-    earlier = jnp.cumsum(onehot, axis=0) - onehot
-    slot_rank = jnp.sum(earlier * onehot, axis=1)
-    position = flat_routes * capacity + slot_rank
-    owner_row = jnp.arange(row_count * pick_count, dtype=jnp.int32) // pick_count
-    slot_token = jnp.full((experts * capacity,), row_count, jnp.int32).at[position].set(owner_row)
-    return (position.reshape(row_count, pick_count), slot_token)
+    )(own, queries, forget, whole, later)
+
+
+MESH = pl.DeviceIdType.MESH
+EXPERTS = 32
+SLOTS = 32
+TOKENS = 128
+WIDTH = 2048
+PART = 256
+ALL_SLOTS = EXPERTS * SLOTS
+CHUNKS = 4
+CHUNK = ALL_SLOTS // CHUNKS
+PER_CHUNK = CHUNK // SLOTS
+HALF = CHUNK // 2
+
+
+def offset_at(position):
+    return (position + 1) // 2 if position % 2 else (EXPERTS - position // 2) % EXPERTS
+
+
+def mirror(position):
+    if position in (0, EXPERTS - 1):
+        return position
+    return position + 1 if position % 2 else position - 1
+
+
+def landed(ref, sem):
+    pltpu.make_async_copy(ref, ref, sem).wait()
+
+
+def moe_kernel(
+    tokens,
+    gain,
+    routes,
+    logits,
+    gate_hbm,
+    up_hbm,
+    down_hbm,
+    out,
+    gate,
+    up,
+    down,
+    place,
+    weigh,
+    outgoing,
+    features,
+    partial,
+    paired,
+    passed,
+    reached,
+    result,
+    returned,
+    load_sem,
+    go_send,
+    go_recv,
+    ag_send,
+    ag_recv,
+    rs_send,
+    rs_recv,
+    back_send,
+    back_recv,
+):
+    z, x, t = lax.axis_index("ep_0"), lax.axis_index("ep_1"), lax.axis_index("tp")
+    me = z * 4 + x
+    y, core = t // 2, t % 2
+    above = ((y + 1) % 4) * 2 + core
+    below = ((y + 3) % 4) * 2 + core
+    across = ((y + 2) % 4) * 2 + core
+    beside = y * 2 + (1 - core)
+
+    def twin(number):
+        return (number // 2) * 2 + 1 - core
+
+    def along(offset):
+        peer = (me + offset) % EXPERTS
+        return {"ep_0": peer // 4, "ep_1": peer % 4}
+
+    barrier = pltpu.get_barrier_semaphore()
+    for offset in range(1, EXPERTS):
+        pl.semaphore_signal(barrier, inc=1, device_id=along(offset), device_id_type=MESH)
+    for offset in range(1, 8):
+        pl.semaphore_signal(
+            barrier, inc=1, device_id={"tp": (t + offset) % 8}, device_id_type=MESH
+        )
+    loads = [
+        pltpu.make_async_copy(source, target, load_sem.at[number])
+        for number, (source, target) in enumerate(((gate_hbm, gate), (up_hbm, up), (down_hbm, down)))
+    ]
+    for load in loads:
+        load.start()
+
+    values = tokens[...].astype(jnp.float32)
+    inverse = lax.rsqrt(jnp.mean(values * values, axis=1, keepdims=True) + epsilon)
+    columns = pl.ds(pl.multiple_of(t * PART, PART), PART)
+    own = (tokens[:, columns].astype(jnp.float32) * inverse * gain[:, columns]).astype(
+        jnp.bfloat16
+    )
+    picks = routes[...]
+    raised = jnp.exp(logits[...] - jnp.max(logits[...], axis=0, keepdims=True))
+    route_weight = raised / jnp.sum(raised, axis=0, keepdims=True)
+    number = lax.broadcasted_iota(jnp.int32, (EXPERTS, TOKENS), 0)
+    offset = jnp.where(number % 2 == 1, (number + 1) // 2, (EXPERTS - number // 2) % EXPERTS)
+    expert = (me + offset) % EXPERTS
+    named = jnp.zeros((EXPERTS, TOKENS), jnp.float32)
+    share = jnp.zeros((EXPERTS, TOKENS), jnp.float32)
+    for pick in range(4):
+        same = picks[pick : pick + 1, :] == expert
+        named = named + jnp.where(same, 1.0, 0.0)
+        share = share + jnp.where(same, route_weight[pick : pick + 1, :], 0.0)
+    before = (
+        lax.broadcasted_iota(jnp.int32, (TOKENS, TOKENS), 0)
+        < lax.broadcasted_iota(jnp.int32, (TOKENS, TOKENS), 1)
+    )
+    rank = jnp.dot(
+        named.astype(jnp.bfloat16),
+        jnp.where(before, 1.0, 0.0).astype(jnp.bfloat16),
+        preferred_element_type=jnp.float32,
+    )
+    slot = jnp.where(named > 0.0, rank, -1.0)
+    share_high = share.astype(jnp.bfloat16).astype(jnp.float32)
+    share_low = share - share_high
+    level = lax.broadcasted_iota(jnp.int32, (SLOTS, TOKENS), 0).astype(jnp.float32)
+    for position in range(EXPERTS):
+        hit = level == slot[position : position + 1, :]
+        rows = slice(position * SLOTS, (position + 1) * SLOTS)
+        place[rows, :] = jnp.where(hit, 1.0, 0.0).astype(jnp.bfloat16)
+        weigh[0, rows, :] = jnp.where(hit, share_high[position : position + 1, :], 0.0).astype(
+            jnp.bfloat16
+        )
+        weigh[1, rows, :] = jnp.where(hit, share_low[position : position + 1, :], 0.0).astype(
+            jnp.bfloat16
+        )
+    outgoing[...] = jnp.dot(place[...], own, preferred_element_type=jnp.float32).astype(
+        jnp.bfloat16
+    )
+    features[t, 0:SLOTS, :] = outgoing[0:SLOTS, :]
+    pl.semaphore_wait(barrier, EXPERTS - 1 + 7)
+
+    started = []
+
+    def send(source, target, send_sem, recv_sem, device):
+        copy = pltpu.make_async_remote_copy(
+            src_ref=source,
+            dst_ref=target,
+            send_sem=send_sem,
+            recv_sem=recv_sem,
+            device_id=device,
+            device_id_type=MESH,
+        )
+        copy.start()
+        started.append(copy)
+
+    def slots(position):
+        return pl.ds(position * SLOTS, SLOTS)
+
+    for position in range(1, EXPERTS):
+        landing = mirror(position)
+        send(
+            outgoing.at[slots(position)],
+            features.at[t, slots(landing)],
+            go_send.at[position],
+            go_recv.at[landing],
+            along(offset_at(position)),
+        )
+
+    def rows_of(chunk):
+        return pl.ds(chunk * CHUNK, CHUNK)
+
+    def spread(chunk):
+        for position in range(chunk * PER_CHUNK, (chunk + 1) * PER_CHUNK):
+            if position:
+                landed(features.at[t, slots(position)], go_recv.at[position])
+        block = features.at[t, rows_of(chunk)]
+        for kind, target in ((0, above), (1, below), (4, beside)):
+            send(block, block, ag_send.at[chunk, kind], ag_recv.at[chunk, kind], {"tp": target})
+
+    def forward(chunk):
+        for kind, source, target, first in ((0, below, above, 0), (1, above, below, HALF)):
+            block = features.at[source, rows_of(chunk)]
+            landed(block, ag_recv.at[chunk, kind])
+            part = features.at[source, pl.ds(chunk * CHUNK + first, HALF)]
+            send(part, part, ag_send.at[chunk, 2 + kind], ag_recv.at[chunk, 2 + kind], {"tp": target})
+            send(block, block, ag_send.at[chunk, 5 + kind], ag_recv.at[chunk, 5 + kind], {"tp": beside})
+
+    def complete(chunk):
+        for kind, first in ((2, 0), (3, HALF)):
+            landed(
+                features.at[across, pl.ds(chunk * CHUNK + first, HALF)], ag_recv.at[chunk, kind]
+            )
+        block = features.at[across, rows_of(chunk)]
+        send(block, block, ag_send.at[chunk, 7], ag_recv.at[chunk, 7], {"tp": beside})
+
+    def multiply(chunk):
+        for kind, source in ((4, beside), (5, twin(below)), (6, twin(above)), (7, twin(across))):
+            landed(features.at[source, rows_of(chunk)], ag_recv.at[chunk, kind])
+        if chunk == 0:
+            for load in loads:
+                load.wait()
+        gate_sum = jnp.zeros((CHUNK, PART), jnp.float32)
+        up_sum = jnp.zeros((CHUNK, PART), jnp.float32)
+        for source in range(8):
+            rows = features[source, rows_of(chunk), :]
+            depth = slice(source * PART, (source + 1) * PART)
+            gate_sum = gate_sum + jnp.dot(rows, gate[depth, :], preferred_element_type=jnp.float32)
+            up_sum = up_sum + jnp.dot(rows, up[depth, :], preferred_element_type=jnp.float32)
+        gate_cut = jnp.minimum(gate_sum, clamp_limit)
+        up_cut = jnp.clip(up_sum, -clamp_limit, clamp_limit)
+        hidden = ((up_cut + 1.0) * gate_cut * jax.nn.sigmoid(sigmoid_slope * gate_cut)).astype(
+            jnp.bfloat16
+        )
+        for other in (1, 0):
+            for turn in range(4):
+                target = ((y + turn) % 4) * 2 + ((1 - core) if other else core)
+                partial[chunk, other, turn] = jnp.dot(
+                    hidden,
+                    down[:, pl.ds(pl.multiple_of(target * PART, PART), PART)],
+                    preferred_element_type=jnp.float32,
+                ).astype(jnp.bfloat16)
+            if other:
+                send(
+                    partial.at[chunk, 1],
+                    paired.at[chunk],
+                    rs_send.at[chunk, 0],
+                    rs_recv.at[chunk, 0],
+                    {"tp": beside},
+                )
+
+    def added(*values):
+        total = values[0].astype(jnp.float32)
+        for value in values[1:]:
+            total = total + value.astype(jnp.float32)
+        return total.astype(jnp.bfloat16)
+
+    def join(chunk):
+        landed(paired.at[chunk], rs_recv.at[chunk, 0])
+        partial[chunk, 0, 2] = added(partial[chunk, 0, 2], paired[chunk, 2])
+        for kind, first, target in ((1, 0, above), (2, HALF, below)):
+            send(
+                partial.at[chunk, 0, 2, pl.ds(first, HALF)],
+                passed.at[chunk, kind - 1],
+                rs_send.at[chunk, kind],
+                rs_recv.at[chunk, kind],
+                {"tp": target},
+            )
+        for turn in (1, 3, 0):
+            partial[chunk, 0, turn] = added(partial[chunk, 0, turn], paired[chunk, turn])
+
+    def pass_on(chunk):
+        for kind, turn, first, target in ((1, 1, 0, above), (2, 3, HALF, below)):
+            landed(passed.at[chunk, kind - 1], rs_recv.at[chunk, kind])
+            rows = slice(first, first + HALF)
+            partial[chunk, 0, turn, rows] = added(
+                partial[chunk, 0, turn, rows], passed[chunk, kind - 1]
+            )
+            send(
+                partial.at[chunk, 0, turn],
+                reached.at[chunk, kind - 1],
+                rs_send.at[chunk, 2 + kind],
+                rs_recv.at[chunk, 2 + kind],
+                {"tp": target},
+            )
+
+    def finish(chunk):
+        for kind in (3, 4):
+            landed(reached.at[chunk, kind - 3], rs_recv.at[chunk, kind])
+        result[rows_of(chunk), :] = added(
+            partial[chunk, 0, 0], reached[chunk, 0], reached[chunk, 1]
+        )
+        for position in range(chunk * PER_CHUNK, (chunk + 1) * PER_CHUNK):
+            if position == 0:
+                returned[0:SLOTS, :] = result[0:SLOTS, :]
+                continue
+            landing = mirror(position)
+            send(
+                result.at[slots(position)],
+                returned.at[slots(landing)],
+                back_send.at[position],
+                back_recv.at[landing],
+                along(offset_at(position)),
+            )
+
+    plan = (
+        (spread, 0), (spread, 1), (forward, 0), (spread, 2), (forward, 1), (complete, 0),
+        (multiply, 0), (spread, 3), (forward, 2), (complete, 1), (join, 0), (multiply, 1),
+        (forward, 3), (complete, 2), (pass_on, 0), (join, 1), (multiply, 2), (complete, 3),
+        (finish, 0), (pass_on, 1), (join, 2), (multiply, 3), (finish, 1), (pass_on, 2),
+        (join, 3), (finish, 2), (pass_on, 3), (finish, 3),
+    )
+    for step, chunk in plan:
+        step(chunk)
+    for position in range(1, EXPERTS):
+        landed(returned.at[slots(position)], back_recv.at[position])
+    turned = (((0,), (0,)), ((), ()))
+    out[...] = (
+        lax.dot_general(weigh[0], returned[...], turned, preferred_element_type=jnp.float32)
+        + lax.dot_general(weigh[1], returned[...], turned, preferred_element_type=jnp.float32)
+    ).astype(jnp.bfloat16)
+    for copy in started:
+        copy.wait_send()
+
+
+def experts(tokens, gain, routes, logits, gate, up, down):
+    vmem = pl.BlockSpec(memory_space=pltpu.VMEM)
+    anywhere = pl.BlockSpec(memory_space=pl.ANY)
+    half = jnp.bfloat16
+    dma = pltpu.SemaphoreType.DMA
+    return pl.pallas_call(
+        moe_kernel,
+        out_shape=jax.ShapeDtypeStruct((TOKENS, PART), half),
+        in_specs=[vmem] * 4 + [anywhere] * 3,
+        out_specs=vmem,
+        scratch_shapes=[
+            pltpu.VMEM((WIDTH, PART), half),
+            pltpu.VMEM((WIDTH, PART), half),
+            pltpu.VMEM((PART, WIDTH), half),
+            pltpu.VMEM((ALL_SLOTS, TOKENS), half),
+            pltpu.VMEM((2, ALL_SLOTS, TOKENS), half),
+            pltpu.VMEM((ALL_SLOTS, PART), half),
+            pltpu.VMEM((8, ALL_SLOTS, PART), half),
+            pltpu.VMEM((CHUNKS, 2, 4, CHUNK, PART), half),
+            pltpu.VMEM((CHUNKS, 4, CHUNK, PART), half),
+            pltpu.VMEM((CHUNKS, 2, HALF, PART), half),
+            pltpu.VMEM((CHUNKS, 2, CHUNK, PART), half),
+            pltpu.VMEM((ALL_SLOTS, PART), half),
+            pltpu.VMEM((ALL_SLOTS, PART), half),
+            dma((3,)),
+            dma((EXPERTS,)),
+            dma((EXPERTS,)),
+            dma((CHUNKS, 8)),
+            dma((CHUNKS, 8)),
+            dma((CHUNKS, 5)),
+            dma((CHUNKS, 5)),
+            dma((EXPERTS,)),
+            dma((EXPERTS,)),
+        ],
+        compiler_params=pltpu.CompilerParams(
+            collective_id=0, has_side_effects=True, vmem_limit_bytes=48 * 2**20
+        ),
+        cost_estimate=pl.CostEstimate(
+            flops=4 * 10**10, bytes_accessed=2**23, transcendentals=10**6
+        ),
+    )(tokens, gain, routes, logits, gate, up, down)
 
 
 def body(
@@ -185,54 +507,20 @@
     down_weight,
 ):
     whole = gathered_by_axis(keys_values, EP, 0)
+    moe_out = experts(
+        expert_tokens,
+        expert_gain.reshape(1, -1),
+        routes.T,
+        route_logits.T,
+        gate_weight[0],
+        up_weight[0],
+        down_weight[0],
+    )
     own = lax.axis_index(EP).astype(jnp.int32).reshape(1)
-    attended = attention(own, queries, forget_cache, whole)
+    attended = attention(own, queries, forget_cache, whole, moe_out)
     local_rows = lax.all_to_all(attended, "tp", split_axis=0, concat_axis=1, tiled=True)
     heads_normed = scaled_rows(local_rows, heads_gain)
     mixer_out = jnp.dot(heads_normed, output_weight, preferred_element_type=jnp.float32).astype(
-        jnp.bfloat16
-    )
-    experts_count = lax.axis_size(EP)
-    expert_rows, pick_count = routes.shape
-    capacity = 2 * expert_rows * pick_count // experts_count
-    expert_in = scaled_rows(expert_tokens, expert_gain)
-    shifted = route_logits - jnp.max(route_logits, axis=1, keepdims=True)
-    raised = jnp.exp(shifted)
-    route_weight = raised / jnp.sum(raised, axis=1, keepdims=True)
-    position, slot_token = assign_slots(routes, experts_count, capacity)
-    model_width = expert_in.shape[1]
-    part_width = model_width // lax.axis_size("tp")
-    gate_local = gate_weight[0]
-    up_local = up_weight[0]
-    down_local = down_weight[0]
-    own_columns = lax.dynamic_slice_in_dim(
-        expert_in, lax.axis_index("tp") * part_width, part_width, 1
-    )
-    padded = jnp.concatenate([own_columns, jnp.zeros((1, part_width), jnp.bfloat16)], axis=0)
-    outgoing = jnp.take(padded, slot_token, axis=0).reshape(experts_count, capacity, part_width)
-    arrived = lax.all_to_all(outgoing, EP, split_axis=0, concat_axis=0, tiled=True).reshape(
-        experts_count * capacity, part_width
-    )
-    piece_rows = lax.all_gather(arrived, "tp", axis=1, tiled=True)
-    gate_sum = jnp.dot(piece_rows, gate_local, preferred_element_type=jnp.float32)
-    up_sum = jnp.dot(piece_rows, up_local, preferred_element_type=jnp.float32)
-    gate_cut = jnp.minimum(gate_sum, clamp_limit)
-    up_cut = jnp.clip(up_sum, -clamp_limit, clamp_limit)
-    hidden = ((up_cut + 1.0) * gate_cut * jax.nn.sigmoid(sigmoid_slope * gate_cut)).astype(
-        jnp.bfloat16
-    )
-    expert_out = sent_and_summed(
-        lax.dot_general(
-            down_local, hidden, (((0,), (1,)), ((), ())), preferred_element_type=jnp.float32
-        ).astype(jnp.bfloat16),
-        "tp",
-        0,
-    ).astype(jnp.bfloat16)
-    returned = lax.all_to_all(expert_out, EP, split_axis=1, concat_axis=1, tiled=True)
-    picked = jnp.take(returned, position.reshape(-1), axis=1).reshape(
-        part_width, expert_rows, pick_count
-    )
-    moe_out = jnp.einsum("crk,rk->rc", picked.astype(jnp.float32), route_weight).astype(
         jnp.bfloat16
     )
     return (mixer_out, moe_out)

time: 210 us -> 142 us (0.68)
  the two profiles are of different devices: /device:TPU:2 before, /device:TPU:230 now
where the time goes in v2:
time: 142 us; the launch traced here: 141 us
  Pallas kernels  92 us (65%)
  blocking collectives  23.8 us (17%)
  between operations  14.1 us (10%)
  local copies, waits for them, and re-layouts  9.59 us (7%)
  matrix products  1.61 us (1%)
    pallas_call x1, Pallas kernels, experts(): pl.pallas_call(moe_kernel, out_shape=jax.ShapeDtypeStruct((TOKENS, PART),...  69.5 us
    pallas_call x1, Pallas kernels, attention(): pl.pallas_call(attention_kernel, out_shape=jax.ShapeDtypeStruct((ROWS, 2...  22.5 us
    all_gather x1, blocking collectives, gathered_by_axis(): whole = lax.all_gather(whole, axes[number], axis=dim, tiled=True)  13.7 us
    all_to_all x1, blocking collectives, body(): lax.all_to_all(attended, 'tp', split_axis=0, concat_axis=1, tiled=True)  10.1 us
    unnamed x25, local copies, waits for them, and re-layouts  9.59 us
  transfers between devices with their start and end apart: 1, of which 0 were waited for; matrix products, arithmetic and copies ran while one was open for 0% of the time, Pallas kernels for 49%

profile of v2, /device:TPU:230, one launch (start us, length us, event | category | flops | bytes accessed | tf_op | source)
XLA Modules:
  0.0 141.4 jit_solution(10410275416754331116)
XLA Ops:
  7.2 0.0 all-gather.2.cloned.1.call-start
  7.2 13.7 %all_gather.6 = bf16[2048,128]{1,0:T(8,128)(2,1)} all-gather(bf16[512,128]{1,0:T(8,128)(2,1)} %param.13), channel_id=1, replica_groups=mesh['ep_0'=8,'ep_1'=4,'tp'=8] {'ep_1'}, dimensions={0}, use_global_device_ids=true | all-gather | bytes 655360 | tf_op jit(solution)/shard_map/all_gather | solution.py:24
  20.9 0.0 all-gather.2.cloned.1.call-update
  21.0 0.0 copy-start.1
  21.0 1.2 copy-done.1
  22.2 0.0 copy-start.2
  22.2 1.2 copy-done.2
  23.4 0.0 copy-start.3
  23.4 1.2 copy-done.3
  24.7 0.0 copy-start.4
  24.7 1.0 copy-done.4
  25.7 0.7 copy-done.7
  26.4 0.0 copy-start.8
  26.4 0.7 copy-done.8
  27.1 0.0 copy-start.9
  27.1 0.7 copy-done.9
  27.8 0.0 copy-start.5
  27.8 0.0 copy-start.6
  27.8 69.5 %shard_map.131.later_ref = bf16[128,256]{1,0:T(8,128)(2,1)S(1)} custom-call(bf16[128,2048]{1,0:T(8,128)(2,1)S(1)} %copy-done.4, f32[1,2048]{1,0:T(1,128)S(1)} %bitcast.25, s32[4,128]{1,0:T(4,128)S(1)} %bitcast.26, f32[4,128]{1,0:T(4,128)S(1)} %bitcast.27, bf16[2048,256]{1,0:T(8,128)(2,1)S(1)} %bitcast.22, bf16[2048,256]{1,0:T(8,128)(2,1)S(1)} %bitcast.23, ...), custom_call_target="tpu_custom_call" | custom-call | flops 40000000000 | bytes 8388608 | tf_op jit(solution)/shard_map/pallas_call | solution.py:457
  97.3 0.0 all-gather.2.cloned.1.call-done.kv_ref
  97.3 0.0 copy-done.5
  97.3 0.0 copy-done.6
  97.3 0.0 copy-start
  97.3 2.2 %copy-done = bf16[16384,128]{1,0:T(8,128)(2,1)S(1)} copy-done((bf16[16384,128]{1,0:T(8,128)(2,1)S(1)}, bf16[16384,128]{1,0:T(8,128)(2,1)}, u32[]{:S(2)}) %copy-start) | copy-done | bytes 4194328
  99.5 0.0 copy-start.10
  99.5 22.5 %shard_map.132 = bf16[512,128]{1,0:T(8,128)(2,1)S(1)} custom-call(s32[1]{0:T(128)} %bitcast.own_ref, bf16[512,128]{1,0:T(8,128)(2,1)S(1)} %copy-done.5, f32[2,16384]{1,0:T(2,128)S(1)} %copy-done.6, bf16[16384,128]{1,0:T(8,128)(2,1)S(1)} %copy-done, bf16[128,256]{1,0:T(8,128)(2,1)S(1)} %shard_map.131.later_ref), custom_call_target="tpu_custom_call" | custom-call | flops 10000000000 | bytes 5242880 | tf_op jit(solution)/shard_map/pallas_call | solution.py:130
  122.0 10.1 %all_to_all.13 = bf16[8,64,128]{2,1,0:T(8,128)(2,1)S(1)} all-to-all(bf16[8,64,128]{2,1,0:T(8,128)(2,1)S(1)} %bitcast.21), channel_id=1, replica_groups=mesh['ep_0'=8,'ep_1'=4,'tp'=8] {'tp'}, dimensions={0} | all-to-all | bytes 262144 | tf_op jit(solution)/shard_map/all_to_all | solution.py:521
  132.1 0.1 fusion
  132.3 0.0 copy-done.10
  132.3 0.0 copy-done.11
  132.3 1.6 %convolution_convert_fusion = bf16[64,2048]{1,0:T(8,128)(2,1)} fusion(bf16[1024,2048]{1,0:T(8,128)(2,1)S(1)} %copy-done.10, f32[1024]{0:T(1024)S(1)} %copy-done.11, f32[64]{0:T(128)S(1)} %add_rsqrt_fusion, bf16[8,64,128]{2,1,0:T(8,128)(2,1)S(1)} %all_to_all.13), kind=kOutput, calls=%fused_computation | convolution fusion | flops 268828672 | bytes 4591872 | tf_op jit(solution)/shard_map/dot_general | solution.py:523
  133.9 0.6 copy.20
  (3 shorter events, 0.0 us)
Async XLA Ops:
  7.2 90.1 %all-gather.2.cloned.1.call-start = ((), (), s32[]{:S(2)}) async-start(), calls=%async_computation.1 | async-start | bytes 4718592 | tf_op jit(solution)/shard_map/all_gather | solution.py:24
  21.0 1.2 copy-start.1
  22.2 1.2 copy-start.2
  23.4 1.2 copy-start.3
  24.7 1.0 copy-start.4
  25.7 0.7 copy-start.7
  26.4 0.7 copy-start.8
  27.1 0.7 copy-start.9
  27.8 69.5 %copy-start.5 = (bf16[512,128]{1,0:T(8,128)(2,1)S(1)}, bf16[512,128]{1,0:T(8,128)(2,1)}, u32[]{:S(2)}) copy-start(bf16[512,128]{1,0:T(8,128)(2,1)} %q_ref.1) | copy-start | bytes 393220
  27.8 69.6 %copy-start.6 = (f32[2,16384]{1,0:T(2,128)S(1)}, f32[2,16384]{1,0:T(2,128)}, u32[]{:S(2)}) copy-start(f32[2,16384]{1,0:T(2,128)} %f_ref.1) | copy-start | bytes 393220
  97.3 2.2 %copy-start = (bf16[16384,128]{1,0:T(8,128)(2,1)S(1)}, bf16[16384,128]{1,0:T(8,128)(2,1)}, u32[]{:S(2)}) copy-start(bf16[16384,128]{1,0:T(8,128)(2,1)} %all-gather.2.cloned.1.call-done.kv_ref) | copy-start | bytes 12582916
  99.5 32.8 %copy-start.10 = (bf16[1024,2048]{1,0:T(8,128)(2,1)S(1)}, bf16[1024,2048]{1,0:T(8,128)(2,1)}, u32[]{:S(2)}) copy-start(bf16[1024,2048]{1,0:T(8,128)(2,1)} %param.16) | copy-start | bytes 12582916
  99.5 32.8 %copy-start.11 = (f32[1024]{0:T(1024)S(1)}, f32[1024]{0:T(1024)}, u32[]{:S(2)}) copy-start(f32[1024]{0:T(1024)} %param.15) | copy-start | bytes 12292
Sparse Core Ops, SparseCore 0:
  21.1 74.7 all-gather.1

commit v3 on v2

--- a/solution.py
+++ b/solution.py
@@ -3,9 +3,9 @@
 import jax
 import jax.numpy as jnp
 from jax import lax
-from jax.sharding import Mesh
 from jax.experimental import pallas as pl
 from jax.experimental.pallas import tpu as pltpu
+from jax.sharding import Mesh
 from jax.sharding import PartitionSpec as P
 
 HEAD = 64
@@ -16,19 +16,6 @@
 epsilon = 1e-06
 clamp_limit = 7.0
 sigmoid_slope = 1.702
-
-
-def gathered_by_axis(array, axes, dim):
-    whole = array
-    for number in range(len(axes) - 1, -1, -1):
-        whole = lax.all_gather(whole, axes[number], axis=dim, tiled=True)
-    return whole
-
-
-def scaled_rows(values, gain_vector):
-    as_float = values.astype(jnp.float32)
-    inverse = lax.rsqrt(jnp.mean(as_float * as_float, axis=-1, keepdims=True) + epsilon)
-    return (as_float * inverse * gain_vector).astype(jnp.bfloat16)
 
 
 def split3(x):
@@ -70,85 +57,6 @@
 def value_operand(block_rows):
     turned = block_rows.astype(jnp.float32).T[HEAD : 2 * HEAD].astype(jnp.bfloat16)
     return jnp.concatenate([turned, jnp.ones((16, ROWS), jnp.bfloat16)], axis=0)
-
-
-def attention_kernel(own_ref, q_ref, f_ref, kv_ref, later_ref, o_ref, qx, top, acc, s_ref):
-    own = own_ref[0]
-    query_operand(q_ref[...], qx)
-    base = pl.multiple_of(own * ROWS, ROWS)
-    start = f_ref[:, pl.ds(base, 128)][:, 0:1]
-    top[...] = jnp.full_like(top, -jnp.inf)
-    acc[...] = jnp.zeros_like(acc)
-
-    def rows_of(block):
-        return pl.ds(pl.multiple_of(block * ROWS, ROWS), ROWS)
-
-    keys = key_operand(kv_ref[rows_of(own), :], f_ref[:, rows_of(own)] - start)
-    for tile in range(ASKED // TILE):
-        cut = slice(tile * TILE, (tile + 1) * TILE)
-        scores = jnp.dot(keys, qx[:, cut], preferred_element_type=jnp.float32)
-        key_at = lax.broadcasted_iota(jnp.int32, (ROWS, TILE), 0)
-        query_at = lax.broadcasted_iota(jnp.int32, (ROWS, TILE), 1) + (tile * TILE) % ROWS
-        s_ref[0, :, cut] = jnp.where(key_at <= query_at, scores, -jnp.inf)
-
-    def take(block, after, slot):
-        keys = key_operand(kv_ref[rows_of(after), :], f_ref[:, rows_of(after)] - start)
-        values = value_operand(kv_ref[rows_of(block), :])
-        for tile in range(ASKED // TILE):
-            cut = slice(tile * TILE, (tile + 1) * TILE)
-            s_ref[1 - slot, :, cut] = jnp.dot(
-                keys, qx[:, cut], preferred_element_type=jnp.float32
-            )
-            scores = s_ref[slot, :, cut]
-            old = top[:, cut]
-            new = jnp.maximum(old, jnp.max(scores, axis=0, keepdims=True))
-            weights = jnp.exp(scores - new).astype(jnp.bfloat16)
-            acc[:, cut] = acc[:, cut] * jnp.exp(old - new) + jnp.dot(
-                values, weights, preferred_element_type=jnp.float32
-            )
-            top[:, cut] = new
-
-    def pair(step, _):
-        first = 2 * step
-        take(jnp.where(first == 0, own, first - 1), jnp.minimum(first, jnp.maximum(own - 1, 0)), 0)
-
-        @pl.when(first + 1 <= own)
-        def _():
-            take(first, jnp.minimum(first + 1, own - 1), 1)
-
-        return 0
-
-    lax.fori_loop(0, (own + 2) // 2, pair, 0)
-    total = acc[...]
-    result = total[0:HEAD] / total[HEAD : HEAD + 1]
-    both = jnp.concatenate([result[:, 0:ROWS], result[:, ROWS:ASKED]], axis=0)
-    o_ref[...] = both.T.astype(jnp.bfloat16)
-
-
-def attention(own, queries, forget, whole, later):
-    vmem = pl.BlockSpec(memory_space=pltpu.VMEM)
-    return pl.pallas_call(
-        attention_kernel,
-        out_shape=jax.ShapeDtypeStruct((ROWS, 2 * HEAD), jnp.bfloat16),
-        in_specs=[
-            pl.BlockSpec(memory_space=pltpu.SMEM),
-            vmem,
-            vmem,
-            vmem,
-            pl.BlockSpec(memory_space=pl.ANY),
-        ],
-        out_specs=vmem,
-        scratch_shapes=[
-            pltpu.VMEM((2 * HEAD, ASKED), jnp.bfloat16),
-            pltpu.VMEM((1, ASKED), jnp.float32),
-            pltpu.VMEM((HEAD + 16, ASKED), jnp.float32),
-            pltpu.VMEM((2, ROWS, ASKED), jnp.float32),
-        ],
-        compiler_params=pltpu.CompilerParams(vmem_limit_bytes=40 * 2**20),
-        cost_estimate=pl.CostEstimate(
-            flops=10**10, bytes_accessed=5 * 2**20, transcendentals=10**7
-        ),
-    )(own, queries, forget, whole, later)
 
 
 MESH = pl.DeviceIdType.MESH
@@ -162,6 +70,10 @@
 CHUNK = ALL_SLOTS // CHUNKS
 PER_CHUNK = CHUNK // SLOTS
 HALF = CHUNK // 2
+PLANES = 8
+FIRST = 320
+SECOND = ROWS - FIRST
+SHARE = ROWS // 8
 
 
 def offset_at(position):
@@ -178,7 +90,7 @@
     pltpu.make_async_copy(ref, ref, sem).wait()
 
 
-def moe_kernel(
+def kernel(
     tokens,
     gain,
     routes,
@@ -186,7 +98,13 @@
     gate_hbm,
     up_hbm,
     down_hbm,
+    queries,
+    forget,
+    heads_gain,
+    own_hbm,
+    mix_hbm,
     out,
+    mixer_out,
     gate,
     up,
     down,
@@ -200,6 +118,14 @@
     reached,
     result,
     returned,
+    mix,
+    keys,
+    qx,
+    top,
+    acc,
+    s_ref,
+    attended,
+    gathered,
     load_sem,
     go_send,
     go_recv,
@@ -209,6 +135,16 @@
     rs_recv,
     back_send,
     back_recv,
+    az_send,
+    az_recv,
+    ax_send,
+    ax_recv,
+    bx_send,
+    bx_recv,
+    bz_send,
+    bz_recv,
+    at_send,
+    at_recv,
 ):
     z, x, t = lax.axis_index("ep_0"), lax.axis_index("ep_1"), lax.axis_index("tp")
     me = z * 4 + x
@@ -234,7 +170,15 @@
         )
     loads = [
         pltpu.make_async_copy(source, target, load_sem.at[number])
-        for number, (source, target) in enumerate(((gate_hbm, gate), (up_hbm, up), (down_hbm, down)))
+        for number, (source, target) in enumerate(
+            (
+                (own_hbm, keys.at[me]),
+                (gate_hbm, gate),
+                (up_hbm, up),
+                (down_hbm, down),
+                (mix_hbm, mix),
+            )
+        )
     ]
     for load in loads:
         load.start()
@@ -292,13 +236,13 @@
         copy = pltpu.make_async_remote_copy(
             src_ref=source,
             dst_ref=target,
-            send_sem=send_sem,
+            send_sem=send_sem[0].at[send_sem[1]],
             recv_sem=recv_sem,
             device_id=device,
             device_id_type=MESH,
         )
         copy.start()
-        started.append(copy)
+        started.append((source.shape, send_sem))
 
     def slots(position):
         return pl.ds(position * SLOTS, SLOTS)
@@ -308,7 +252,7 @@
         send(
             outgoing.at[slots(position)],
             features.at[t, slots(landing)],
-            go_send.at[position],
+            (go_send, (position,)),
             go_recv.at[landing],
             along(offset_at(position)),
         )
@@ -322,15 +266,15 @@
                 landed(features.at[t, slots(position)], go_recv.at[position])
         block = features.at[t, rows_of(chunk)]
         for kind, target in ((0, above), (1, below), (4, beside)):
-            send(block, block, ag_send.at[chunk, kind], ag_recv.at[chunk, kind], {"tp": target})
+            send(block, block, (ag_send, (chunk, kind,)), ag_recv.at[chunk, kind], {"tp": target})
 
     def forward(chunk):
         for kind, source, target, first in ((0, below, above, 0), (1, above, below, HALF)):
             block = features.at[source, rows_of(chunk)]
             landed(block, ag_recv.at[chunk, kind])
             part = features.at[source, pl.ds(chunk * CHUNK + first, HALF)]
-            send(part, part, ag_send.at[chunk, 2 + kind], ag_recv.at[chunk, 2 + kind], {"tp": target})
-            send(block, block, ag_send.at[chunk, 5 + kind], ag_recv.at[chunk, 5 + kind], {"tp": beside})
+            send(part, part, (ag_send, (chunk, 2 + kind,)), ag_recv.at[chunk, 2 + kind], {"tp": target})
+            send(block, block, (ag_send, (chunk, 5 + kind,)), ag_recv.at[chunk, 5 + kind], {"tp": beside})
 
     def complete(chunk):
         for kind, first in ((2, 0), (3, HALF)):
@@ -338,13 +282,13 @@
                 features.at[across, pl.ds(chunk * CHUNK + first, HALF)], ag_recv.at[chunk, kind]
             )
         block = features.at[across, rows_of(chunk)]
-        send(block, block, ag_send.at[chunk, 7], ag_recv.at[chunk, 7], {"tp": beside})
+        send(block, block, (ag_send, (chunk, 7,)), ag_recv.at[chunk, 7], {"tp": beside})
 
     def multiply(chunk):
         for kind, source in ((4, beside), (5, twin(below)), (6, twin(above)), (7, twin(across))):
             landed(features.at[source, rows_of(chunk)], ag_recv.at[chunk, kind])
         if chunk == 0:
-            for load in loads:
+            for load in loads[1:4]:
                 load.wait()
         gate_sum = jnp.zeros((CHUNK, PART), jnp.float32)
         up_sum = jnp.zeros((CHUNK, PART), jnp.float32)
@@ -370,7 +314,7 @@
                 send(
                     partial.at[chunk, 1],
                     paired.at[chunk],
-                    rs_send.at[chunk, 0],
+                    (rs_send, (chunk, 0,)),
                     rs_recv.at[chunk, 0],
                     {"tp": beside},
                 )
@@ -388,7 +332,7 @@
             send(
                 partial.at[chunk, 0, 2, pl.ds(first, HALF)],
                 passed.at[chunk, kind - 1],
-                rs_send.at[chunk, kind],
+                (rs_send, (chunk, kind,)),
                 rs_recv.at[chunk, kind],
                 {"tp": target},
             )
@@ -405,7 +349,7 @@
             send(
                 partial.at[chunk, 0, turn],
                 reached.at[chunk, kind - 1],
-                rs_send.at[chunk, 2 + kind],
+                (rs_send, (chunk, 2 + kind,)),
                 rs_recv.at[chunk, 2 + kind],
                 {"tp": target},
             )
@@ -424,20 +368,205 @@
             send(
                 result.at[slots(position)],
                 returned.at[slots(landing)],
-                back_send.at[position],
+                (back_send, (position,)),
                 back_recv.at[landing],
                 along(offset_at(position)),
             )
 
-    plan = (
-        (spread, 0), (spread, 1), (forward, 0), (spread, 2), (forward, 1), (complete, 0),
-        (multiply, 0), (spread, 3), (forward, 2), (complete, 1), (join, 0), (multiply, 1),
-        (forward, 3), (complete, 2), (pass_on, 0), (join, 1), (multiply, 2), (complete, 3),
-        (finish, 0), (pass_on, 1), (join, 2), (multiply, 3), (finish, 1), (pass_on, 2),
-        (join, 3), (finish, 2), (pass_on, 3), (finish, 3),
-    )
-    for step, chunk in plan:
-        step(chunk)
+    def plane_of(turn):
+        step = (turn + 1) // 2
+        return (z + (8 - step if turn % 2 else step)) % PLANES
+
+    def block_of(turn, side):
+        return plane_of(turn) * 4 + (x + side) % 4
+
+    a_rows = pl.ds(0, FIRST)
+    a_halves = (pl.ds(0, FIRST // 2), pl.ds(FIRST // 2, FIRST // 2))
+    b_rows = pl.ds(FIRST, SECOND)
+    b_halves = (pl.ds(FIRST, SECOND // 2), pl.ds(FIRST + SECOND // 2, SECOND // 2))
+    z_next = ({"ep_0": (z + 1) % PLANES}, {"ep_0": (z + 7) % PLANES})
+    x_next = ({"ep_1": (x + 1) % 4}, {"ep_1": (x + 3) % 4})
+
+    def along_x(turn):
+        piece = keys.at[block_of(turn, 0), a_rows]
+        for way in range(2):
+            send(piece, piece, (ax_send, (turn, way,)), ax_recv.at[turn, way], x_next[way])
+
+    def keys_start():
+        loads[0].wait()
+        piece = keys.at[me, a_rows]
+        for way in range(2):
+            send(piece, piece, (az_send, (way, 0,)), az_recv.at[way, 0], z_next[way])
+        rest = keys.at[me, b_rows]
+        for way in range(2):
+            send(rest, rest, (bx_send, (way,)), bx_recv.at[way], x_next[way])
+        along_x(0)
+
+    def turn_at(step, way):
+        return 7 if step == 4 else 2 * step - 1 + way
+
+    def a_z(step):
+        for way in range(2):
+            block = block_of(turn_at(step, way), 0)
+            rows = a_rows if step < 4 else a_halves[way]
+            landed(keys.at[block, rows], az_recv.at[way, step - 1])
+            if step < 4:
+                piece = keys.at[block, a_rows if step < 3 else a_halves[way]]
+                send(piece, piece, (az_send, (way, step,)), az_recv.at[way, step], z_next[way])
+                along_x(turn_at(step, way))
+        if step == 4:
+            along_x(7)
+
+    def a_x(turn):
+        for way, side in ((0, 3), (1, 1)):
+            block = block_of(turn, side)
+            landed(keys.at[block, a_rows], ax_recv.at[turn, way])
+            piece = keys.at[block, a_halves[way]]
+            send(piece, piece, (ax_send, (turn, 2 + way,)), ax_recv.at[turn, 2 + way], x_next[way])
+
+    def a_done(turn):
+        for way in range(2):
+            landed(keys.at[block_of(turn, 2), a_halves[way]], ax_recv.at[turn, 2 + way])
+
+    def b_x():
+        for way, side in ((0, 3), (1, 1)):
+            block = block_of(0, side)
+            landed(keys.at[block, b_rows], bx_recv.at[way])
+            piece = keys.at[block, b_halves[way]]
+            send(piece, piece, (bx_send, (2 + way,)), bx_recv.at[2 + way], x_next[way])
+
+    def b_row():
+        for way in range(2):
+            landed(keys.at[block_of(0, 2), b_halves[way]], bx_recv.at[2 + way])
+        pieces = keys.at[pl.ds(z * 4, 4), b_rows]
+        for way in range(2):
+            send(pieces, pieces, (bz_send, (way, 0,)), bz_recv.at[way, 0], z_next[way])
+
+    def b_z(step):
+        for way in range(2):
+            blocks = pl.ds(plane_of(turn_at(step, way)) * 4, 4)
+            rows = b_rows if step < 4 else b_halves[way]
+            landed(keys.at[blocks, rows], bz_recv.at[way, step - 1])
+            if step < 4:
+                pieces = keys.at[blocks, b_rows if step < 3 else b_halves[way]]
+                send(pieces, pieces, (bz_send, (way, step,)), bz_recv.at[way, step], z_next[way])
+
+    start = forget[:, pl.ds(pl.multiple_of(me * ROWS, ROWS), 128)][:, 0:1]
+
+    def key_rows(block):
+        gate_rows = pl.ds(pl.multiple_of(block * ROWS, ROWS), ROWS)
+        return key_operand(keys[block], forget[:, gate_rows] - start)
+
+    def own_block():
+        query_operand(queries[...], qx)
+        lanes = key_rows(me)
+        values = value_operand(keys[me])
+        for tile in range(ASKED // TILE):
+            cut = slice(tile * TILE, (tile + 1) * TILE)
+            scores = jnp.dot(lanes, qx[:, cut], preferred_element_type=jnp.float32)
+            key_at = lax.broadcasted_iota(jnp.int32, (ROWS, TILE), 0)
+            query_at = lax.broadcasted_iota(jnp.int32, (ROWS, TILE), 1) + (tile * TILE) % ROWS
+            scores = jnp.where(key_at <= query_at, scores, -jnp.inf)
+            new = jnp.max(scores, axis=0, keepdims=True)
+            weights = jnp.exp(scores - new).astype(jnp.bfloat16)
+            acc[:, cut] = jnp.dot(values, weights, preferred_element_type=jnp.float32)
+            top[:, cut] = new
+
+    def take(block, after, slot):
+        lanes = key_rows(after)
+        values = value_operand(keys[block])
+        for tile in range(ASKED // TILE):
+            cut = slice(tile * TILE, (tile + 1) * TILE)
+            s_ref[1 - slot, :, cut] = jnp.dot(
+                lanes, qx[:, cut], preferred_element_type=jnp.float32
+            )
+            scores = s_ref[slot, :, cut]
+            old = top[:, cut]
+            new = jnp.maximum(old, jnp.max(scores, axis=0, keepdims=True))
+            weights = jnp.exp(scores - new).astype(jnp.bfloat16)
+            acc[:, cut] = acc[:, cut] * jnp.exp(old - new) + jnp.dot(
+                values, weights, preferred_element_type=jnp.float32
+            )
+            top[:, cut] = new
+
+    def attend(first, count):
+        @pl.when(count > 0)
+        def _():
+            lanes = key_rows(first)
+            for tile in range(ASKED // TILE):
+                cut = slice(tile * TILE, (tile + 1) * TILE)
+                s_ref[0, :, cut] = jnp.dot(
+                    lanes, qx[:, cut], preferred_element_type=jnp.float32
+                )
+            last = first + count - 1
+
+            def pair(step, _):
+                block = first + 2 * step
+                take(block, jnp.minimum(block + 1, last), 0)
+
+                @pl.when(block + 1 <= last)
+                def _():
+                    take(block + 1, jnp.minimum(block + 2, last), 1)
+
+                return 0
+
+            lax.fori_loop(0, (count + 1) // 2, pair, 0)
+
+    before_rounds = (
+        (keys_start,), (own_block,), (spread, 0), (spread, 1), (forward, 0), (spread, 2),
+        (forward, 1), (complete, 0), (spread, 3), (multiply, 0), (forward, 2), (a_z, 1), (b_x,),
+        (complete, 1), (join, 0), (multiply, 1), (forward, 3), (a_x, 0), (b_row,), (a_z, 2),
+        (complete, 2), (pass_on, 0), (join, 1), (multiply, 2), (a_x, 1), (a_x, 2), (a_z, 3),
+        (b_z, 1), (complete, 3), (finish, 0), (pass_on, 1), (join, 2), (multiply, 3),
+        (a_done, 0), (a_x, 3), (a_x, 4), (a_z, 4),
+    )
+    rounds = (
+        (),
+        ((finish, 1), (pass_on, 2), (join, 3), (a_done, 1), (b_z, 2)),
+        ((a_x, 5), (a_x, 6), (a_done, 2)),
+        ((finish, 2), (pass_on, 3), (a_x, 7), (a_done, 3)),
+        ((a_done, 4), (b_z, 3)),
+        ((finish, 3), (a_done, 5)),
+        ((a_done, 6), (b_z, 4)),
+        ((a_done, 7),),
+    )
+
+    for step, *at in before_rounds:
+        step(*at)
+
+    def one_round(turn, _):
+        for number, events in enumerate(rounds):
+            if events:
+
+                @pl.when(turn == number)
+                def _(events=events):
+                    for step, *at in events:
+                        step(*at)
+
+        odd = turn % 2
+        step = (turn + 1) // 2
+        plane = jnp.where(odd == 1, z - step, z + step - jnp.where(turn > 0, PLANES, 0))
+        count = jnp.where(turn == 0, x, jnp.where(plane >= 0, 4, 0))
+        attend(jnp.maximum(plane, 0) * 4, count)
+        return 0
+
+    lax.fori_loop(0, PLANES, one_round, 0)
+
+    total = acc[...]
+    heads = total[0:HEAD] / total[HEAD : HEAD + 1]
+    both = jnp.concatenate([heads[:, 0:ROWS], heads[:, ROWS:ASKED]], axis=0)
+    attended[...] = both.T.astype(jnp.bfloat16)
+    for offset in range(1, 8):
+        peer = (t + offset) % 8
+        send(
+            attended.at[pl.ds(pl.multiple_of(peer * SHARE, SHARE), SHARE)],
+            gathered.at[t],
+            (at_send, (offset,)),
+            at_recv.at[8 - offset],
+            {"tp": peer},
+        )
+    gathered[t] = attended[pl.ds(pl.multiple_of(t * SHARE, SHARE), SHARE), :]
+
     for position in range(1, EXPERTS):
         landed(returned.at[slots(position)], back_recv.at[position])
     turned = (((0,), (0,)), ((), ()))
@@ -445,20 +574,53 @@
         lax.dot_general(weigh[0], returned[...], turned, preferred_element_type=jnp.float32)
         + lax.dot_general(weigh[1], returned[...], turned, preferred_element_type=jnp.float32)
     ).astype(jnp.bfloat16)
-    for copy in started:
-        copy.wait_send()
-
-
-def experts(tokens, gain, routes, logits, gate, up, down):
+
+    loads[4].wait()
+    for offset in range(1, 8):
+        landed(gathered.at[(t + offset) % 8], at_recv.at[offset])
+    rows = jnp.concatenate([gathered[source] for source in range(8)], axis=1).astype(jnp.float32)
+    inverse = lax.rsqrt(jnp.mean(rows * rows, axis=1, keepdims=True) + epsilon)
+    normed = (rows * inverse * heads_gain[...]).astype(jnp.bfloat16)
+    mixer_out[...] = jnp.dot(normed, mix[...], preferred_element_type=jnp.float32).astype(
+        jnp.bfloat16
+    )
+
+    for shape, sem in started:
+        if shape[-1] == PART:
+            room = partial.at[0, 0] if len(shape) == 3 else returned.at[pl.ds(0, shape[0])]
+        elif len(shape) == 3:
+            room = keys.at[pl.ds(0, 4), pl.ds(0, shape[1])]
+        else:
+            room = keys.at[0, pl.ds(0, shape[0])]
+        landed(room, sem[0].at[sem[1]])
+
+
+def body(
+    queries,
+    keys_values,
+    forget_cache,
+    heads_gain,
+    output_weight,
+    expert_tokens,
+    expert_gain,
+    routes,
+    route_logits,
+    gate_weight,
+    up_weight,
+    down_weight,
+):
     vmem = pl.BlockSpec(memory_space=pltpu.VMEM)
     anywhere = pl.BlockSpec(memory_space=pl.ANY)
     half = jnp.bfloat16
     dma = pltpu.SemaphoreType.DMA
-    return pl.pallas_call(
-        moe_kernel,
-        out_shape=jax.ShapeDtypeStruct((TOKENS, PART), half),
-        in_specs=[vmem] * 4 + [anywhere] * 3,
-        out_specs=vmem,
+    moe_out, mixer_out = pl.pallas_call(
+        kernel,
+        out_shape=(
+            jax.ShapeDtypeStruct((TOKENS, PART), half),
+            jax.ShapeDtypeStruct((SHARE, WIDTH), half),
+        ),
+        in_specs=[vmem] * 4 + [anywhere] * 3 + [vmem] * 3 + [anywhere] * 2,
+        out_specs=(vmem, vmem),
         scratch_shapes=[
             pltpu.VMEM((WIDTH, PART), half),
             pltpu.VMEM((WIDTH, PART), half),
@@ -473,7 +635,15 @@
             pltpu.VMEM((CHUNKS, 2, CHUNK, PART), half),
             pltpu.VMEM((ALL_SLOTS, PART), half),
             pltpu.VMEM((ALL_SLOTS, PART), half),
-            dma((3,)),
+            pltpu.VMEM((16 * HEAD, WIDTH), half),
+            pltpu.VMEM((4 * PLANES, ROWS, 2 * HEAD), half),
+            pltpu.VMEM((2 * HEAD, ASKED), half),
+            pltpu.VMEM((1, ASKED), jnp.float32),
+            pltpu.VMEM((HEAD + 16, ASKED), jnp.float32),
+            pltpu.VMEM((2, ROWS, ASKED), jnp.float32),
+            pltpu.VMEM((ROWS, 2 * HEAD), half),
+            pltpu.VMEM((8, SHARE, 2 * HEAD), half),
+            dma((5,)),
             dma((EXPERTS,)),
             dma((EXPERTS,)),
             dma((CHUNKS, 8)),
@@ -482,32 +652,21 @@
             dma((CHUNKS, 5)),
             dma((EXPERTS,)),
             dma((EXPERTS,)),
+            dma((2, 4)),
+            dma((2, 4)),
+            dma((PLANES, 4)),
+            dma((PLANES, 4)),
+            dma((4,)),
+            dma((4,)),
+            dma((2, 4)),
+            dma((2, 4)),
+            dma((8,)),
+            dma((8,)),
         ],
         compiler_params=pltpu.CompilerParams(
-            collective_id=0, has_side_effects=True, vmem_limit_bytes=48 * 2**20
+            collective_id=0, has_side_effects=True, vmem_limit_bytes=60 * 2**20
         ),
-        cost_estimate=pl.CostEstimate(
-            flops=4 * 10**10, bytes_accessed=2**23, transcendentals=10**6
-        ),
-    )(tokens, gain, routes, logits, gate, up, down)
-
-
-def body(
-    queries,
-    keys_values,
-    forget_cache,
-    heads_gain,
-    output_weight,
-    expert_tokens,
-    expert_gain,
-    routes,
-    route_logits,
-    gate_weight,
-    up_weight,
-    down_weight,
-):
-    whole = gathered_by_axis(keys_values, EP, 0)
-    moe_out = experts(
+    )(
         expert_tokens,
         expert_gain.reshape(1, -1),
         routes.T,
@@ -515,13 +674,11 @@
         gate_weight[0],
         up_weight[0],
         down_weight[0],
-    )
-    own = lax.axis_index(EP).astype(jnp.int32).reshape(1)
-    attended = attention(own, queries, forget_cache, whole, moe_out)
-    local_rows = lax.all_to_all(attended, "tp", split_axis=0, concat_axis=1, tiled=True)
-    heads_normed = scaled_rows(local_rows, heads_gain)
-    mixer_out = jnp.dot(heads_normed, output_weight, preferred_element_type=jnp.float32).astype(
-        jnp.bfloat16
+        queries,
+        forget_cache,
+        heads_gain.reshape(1, -1),
+        keys_values,
+        output_weight,
     )
     return (mixer_out, moe_out)
 

time: 142 us -> 86.5 us (0.61)
  the two profiles are of different devices: /device:TPU:230 before, /device:TPU:225 now
where the time goes in v3:
time: 86.5 us; the launch traced here: 86.3 us
  Pallas kernels  82.5 us (95%)
  local copies, waits for them, and re-layouts  3.14 us (4%)
    pallas_call x1, Pallas kernels, body(): pl.pallas_call(kernel, out_shape=(jax.ShapeDtypeStruct((TOKENS, PART), ha...  82.5 us
    unnamed x2, local copies, waits for them, and re-layouts  3.14 us

profile of v3, /device:TPU:225, one launch (start us, length us, event | category | flops | bytes accessed | tf_op | source)
XLA Modules:
  0.0 86.3 jit_solution(15818454170610262258)
XLA Ops:
  0.6 82.5 %shard_map.131 = (bf16[128,256]{1,0:T(8,128)(2,1)}, bf16[64,2048]{1,0:T(8,128)(2,1)}) custom-call(bf16[128,2048]{1,0:T(8,128)(2,1)} %tokens.1, f32[1,2048]{1,0:T(1,128)} %bitcast.10, s32[4,128]{1,0:T(4,128)} %bitcast.12, f32[4,128]{1,0:T(4,128)} %bitcast.13, bf16[2048,256]{1,0:T(8,128)(2,1)} %bitcast.7, bf16[2048,256]{1,0:T(8,128)(2,1)} %bitcast.8, ...), custom_call_target="tpu_custom_call" | custom-call | tf_op jit(solution)/shard_map/pallas_call | solution.py:616
  83.2 1.7 %copy.16 = bf16[64,2048]{1,0:T(8,128)(2,1)} copy(bf16[64,2048]{1,0:T(8,128)(2,1)} %get-tuple-element.8) | data formatting | bytes 524288
  84.9 1.5 %copy.17 = bf16[128,256]{1,0:T(8,128)(2,1)} copy(bf16[128,256]{1,0:T(8,128)(2,1)} %get-tuple-element.9) | data formatting | bytes 131072

commit v4 on v3

--- a/solution.py
+++ b/solution.py
@@ -127,23 +127,15 @@
     attended,
     gathered,
     load_sem,
-    go_send,
+    sent,
     go_recv,
-    ag_send,
     ag_recv,
-    rs_send,
     rs_recv,
-    back_send,
     back_recv,
-    az_send,
     az_recv,
-    ax_send,
     ax_recv,
-    bx_send,
     bx_recv,
-    bz_send,
     bz_recv,
-    at_send,
     at_recv,
 ):
     z, x, t = lax.axis_index("ep_0"), lax.axis_index("ep_1"), lax.axis_index("tp")
@@ -230,19 +222,16 @@
     features[t, 0:SLOTS, :] = outgoing[0:SLOTS, :]
     pl.semaphore_wait(barrier, EXPERTS - 1 + 7)
 
-    started = []
-
     def send(source, target, send_sem, recv_sem, device):
         copy = pltpu.make_async_remote_copy(
             src_ref=source,
             dst_ref=target,
-            send_sem=send_sem[0].at[send_sem[1]],
+            send_sem=send_sem,
             recv_sem=recv_sem,
             device_id=device,
             device_id_type=MESH,
         )
         copy.start()
-        started.append((source.shape, send_sem))
 
     def slots(position):
         return pl.ds(position * SLOTS, SLOTS)
@@ -252,8 +241,8 @@
         send(
             outgoing.at[slots(position)],
             features.at[t, slots(landing)],
-            (go_send, (position,)),
-            go_recv.at[landing],
+            sent.at[0],
+            go_recv.at[landing // PER_CHUNK],
             along(offset_at(position)),
         )
 
@@ -261,32 +250,29 @@
         return pl.ds(chunk * CHUNK, CHUNK)
 
     def spread(chunk):
-        for position in range(chunk * PER_CHUNK, (chunk + 1) * PER_CHUNK):
-            if position:
-                landed(features.at[t, slots(position)], go_recv.at[position])
+        first = SLOTS if chunk == 0 else 0
+        landed(
+            features.at[t, pl.ds(chunk * CHUNK + first, CHUNK - first)], go_recv.at[chunk]
+        )
         block = features.at[t, rows_of(chunk)]
-        for kind, target in ((0, above), (1, below), (4, beside)):
-            send(block, block, (ag_send, (chunk, kind,)), ag_recv.at[chunk, kind], {"tp": target})
+        for kind, target in ((0, above), (1, below), (3, beside)):
+            send(block, block, sent.at[1], ag_recv.at[chunk, kind], {"tp": target})
 
     def forward(chunk):
         for kind, source, target, first in ((0, below, above, 0), (1, above, below, HALF)):
             block = features.at[source, rows_of(chunk)]
             landed(block, ag_recv.at[chunk, kind])
             part = features.at[source, pl.ds(chunk * CHUNK + first, HALF)]
-            send(part, part, (ag_send, (chunk, 2 + kind,)), ag_recv.at[chunk, 2 + kind], {"tp": target})
-            send(block, block, (ag_send, (chunk, 5 + kind,)), ag_recv.at[chunk, 5 + kind], {"tp": beside})
+            send(part, part, sent.at[1], ag_recv.at[chunk, 2], {"tp": target})
+            send(block, block, sent.at[1], ag_recv.at[chunk, 3], {"tp": beside})
 
     def complete(chunk):
-        for kind, first in ((2, 0), (3, HALF)):
-            landed(
-                features.at[across, pl.ds(chunk * CHUNK + first, HALF)], ag_recv.at[chunk, kind]
-            )
         block = features.at[across, rows_of(chunk)]
-        send(block, block, (ag_send, (chunk, 7,)), ag_recv.at[chunk, 7], {"tp": beside})
+        landed(block, ag_recv.at[chunk, 2])
+        send(block, block, sent.at[1], ag_recv.at[chunk, 3], {"tp": beside})
 
     def multiply(chunk):
-        for kind, source in ((4, beside), (5, twin(below)), (6, twin(above)), (7, twin(across))):
-            landed(features.at[source, rows_of(chunk)], ag_recv.at[chunk, kind])
+        landed(features.at[pl.ds(0, 4), rows_of(chunk)], ag_recv.at[chunk, 3])
         if chunk == 0:
             for load in loads[1:4]:
                 load.wait()
@@ -314,7 +300,7 @@
                 send(
                     partial.at[chunk, 1],
                     paired.at[chunk],
-                    (rs_send, (chunk, 0,)),
+                    sent.at[2],
                     rs_recv.at[chunk, 0],
                     {"tp": beside},
                 )
@@ -332,7 +318,7 @@
             send(
                 partial.at[chunk, 0, 2, pl.ds(first, HALF)],
                 passed.at[chunk, kind - 1],
-                (rs_send, (chunk, kind,)),
+                sent.at[2],
                 rs_recv.at[chunk, kind],
                 {"tp": target},
             )
@@ -349,14 +335,13 @@
             send(
                 partial.at[chunk, 0, turn],
                 reached.at[chunk, kind - 1],
-                (rs_send, (chunk, 2 + kind,)),
-                rs_recv.at[chunk, 2 + kind],
+                sent.at[2],
+                rs_recv.at[chunk, 3],
                 {"tp": target},
             )
 
     def finish(chunk):
-        for kind in (3, 4):
-            landed(reached.at[chunk, kind - 3], rs_recv.at[chunk, kind])
+        landed(reached.at[chunk], rs_recv.at[chunk, 3])
         result[rows_of(chunk), :] = added(
             partial[chunk, 0, 0], reached[chunk, 0], reached[chunk, 1]
         )
@@ -368,8 +353,8 @@
             send(
                 result.at[slots(position)],
                 returned.at[slots(landing)],
-                (back_send, (position,)),
-                back_recv.at[landing],
+                sent.at[3],
+                back_recv.at[0],
                 along(offset_at(position)),
             )
 
@@ -390,16 +375,16 @@
     def along_x(turn):
         piece = keys.at[block_of(turn, 0), a_rows]
         for way in range(2):
-            send(piece, piece, (ax_send, (turn, way,)), ax_recv.at[turn, way], x_next[way])
+            send(piece, piece, sent.at[4], ax_recv.at[turn, way], x_next[way])
 
     def keys_start():
         loads[0].wait()
         piece = keys.at[me, a_rows]
         for way in range(2):
-            send(piece, piece, (az_send, (way, 0,)), az_recv.at[way, 0], z_next[way])
+            send(piece, piece, sent.at[4], az_recv.at[way, 0], z_next[way])
         rest = keys.at[me, b_rows]
         for way in range(2):
-            send(rest, rest, (bx_send, (way,)), bx_recv.at[way], x_next[way])
+            send(rest, rest, sent.at[4], bx_recv.at[way], x_next[way])
         along_x(0)
 
     def turn_at(step, way):
@@ -412,7 +397,7 @@
             landed(keys.at[block, rows], az_recv.at[way, step - 1])
             if step < 4:
                 piece = keys.at[block, a_rows if step < 3 else a_halves[way]]
-                send(piece, piece, (az_send, (way, step,)), az_recv.at[way, step], z_next[way])
+                send(piece, piece, sent.at[4], az_recv.at[way, step], z_next[way])
                 along_x(turn_at(step, way))
         if step == 4:
             along_x(7)
@@ -422,25 +407,23 @@
             block = block_of(turn, side)
             landed(keys.at[block, a_rows], ax_recv.at[turn, way])
             piece = keys.at[block, a_halves[way]]
-            send(piece, piece, (ax_send, (turn, 2 + way,)), ax_recv.at[turn, 2 + way], x_next[way])
+            send(piece, piece, sent.at[4], ax_recv.at[turn, 2], x_next[way])
 
     def a_done(turn):
-        for way in range(2):
-            landed(keys.at[block_of(turn, 2), a_halves[way]], ax_recv.at[turn, 2 + way])
+        landed(keys.at[block_of(turn, 2), a_rows], ax_recv.at[turn, 2])
 
     def b_x():
         for way, side in ((0, 3), (1, 1)):
             block = block_of(0, side)
             landed(keys.at[block, b_rows], bx_recv.at[way])
             piece = keys.at[block, b_halves[way]]
-            send(piece, piece, (bx_send, (2 + way,)), bx_recv.at[2 + way], x_next[way])
+            send(piece, piece, sent.at[4], bx_recv.at[2], x_next[way])
 
     def b_row():
-        for way in range(2):
-            landed(keys.at[block_of(0, 2), b_halves[way]], bx_recv.at[2 + way])
+        landed(keys.at[block_of(0, 2), b_rows], bx_recv.at[2])
         pieces = keys.at[pl.ds(z * 4, 4), b_rows]
         for way in range(2):
-            send(pieces, pieces, (bz_send, (way, 0,)), bz_recv.at[way, 0], z_next[way])
+            send(pieces, pieces, sent.at[4], bz_recv.at[way, 0], z_next[way])
 
     def b_z(step):
         for way in range(2):
@@ -449,7 +432,7 @@
             landed(keys.at[blocks, rows], bz_recv.at[way, step - 1])
             if step < 4:
                 pieces = keys.at[blocks, b_rows if step < 3 else b_halves[way]]
-                send(pieces, pieces, (bz_send, (way, step,)), bz_recv.at[way, step], z_next[way])
+                send(pieces, pieces, sent.at[4], bz_recv.at[way, step], z_next[way])
 
     start = forget[:, pl.ds(pl.multiple_of(me * ROWS, ROWS), 128)][:, 0:1]
 
@@ -513,22 +496,24 @@
             lax.fori_loop(0, (count + 1) // 2, pair, 0)
 
     before_rounds = (
-        (keys_start,), (own_block,), (spread, 0), (spread, 1), (forward, 0), (spread, 2),
-        (forward, 1), (complete, 0), (spread, 3), (multiply, 0), (forward, 2), (a_z, 1), (b_x,),
-        (complete, 1), (join, 0), (multiply, 1), (forward, 3), (a_x, 0), (b_row,), (a_z, 2),
-        (complete, 2), (pass_on, 0), (join, 1), (multiply, 2), (a_x, 1), (a_x, 2), (a_z, 3),
-        (b_z, 1), (complete, 3), (finish, 0), (pass_on, 1), (join, 2), (multiply, 3),
-        (a_done, 0), (a_x, 3), (a_x, 4), (a_z, 4),
+        (keys_start,), (own_block,), (spread, 0), (spread, 1), (forward, 0), (b_x,), (a_x, 0),
+        (spread, 2), (forward, 1), (complete, 0), (a_z, 1), (b_row,), (spread, 3), (a_done, 0),
+        (a_x, 1), (a_x, 2), (forward, 2), (complete, 1),
     )
     rounds = (
         (),
-        ((finish, 1), (pass_on, 2), (join, 3), (a_done, 1), (b_z, 2)),
-        ((a_x, 5), (a_x, 6), (a_done, 2)),
-        ((finish, 2), (pass_on, 3), (a_x, 7), (a_done, 3)),
-        ((a_done, 4), (b_z, 3)),
-        ((finish, 3), (a_done, 5)),
-        ((a_done, 6), (b_z, 4)),
-        ((a_done, 7),),
+        ((a_z, 2), (b_z, 1), (multiply, 0), (a_done, 1), (a_done, 2)),
+        (
+            (join, 0), (forward, 3), (complete, 2), (a_x, 3), (a_x, 4), (a_z, 3), (multiply, 1),
+        ),
+        (
+            (join, 1), (pass_on, 0), (b_z, 2), (a_x, 5), (a_x, 6), (complete, 3), (a_z, 4),
+            (multiply, 2), (a_done, 3),
+        ),
+        ((pass_on, 1), (finish, 0), (join, 2), (multiply, 3), (a_x, 7), (a_done, 4)),
+        ((b_z, 3), (join, 3), (pass_on, 2), (finish, 1), (a_done, 5)),
+        ((pass_on, 3), (finish, 2), (a_done, 6)),
+        ((b_z, 4), (finish, 3), (a_done, 7)),
     )
 
     for step, *at in before_rounds:
@@ -561,14 +546,13 @@
         send(
             attended.at[pl.ds(pl.multiple_of(peer * SHARE, SHARE), SHARE)],
             gathered.at[t],
-            (at_send, (offset,)),
-            at_recv.at[8 - offset],
+            sent.at[5],
+            at_recv.at[0],
             {"tp": peer},
         )
     gathered[t] = attended[pl.ds(pl.multiple_of(t * SHARE, SHARE), SHARE), :]
 
-    for position in range(1, EXPERTS):
-        landed(returned.at[slots(position)], back_recv.at[position])
+    landed(returned.at[pl.ds(SLOTS, ALL_SLOTS - SLOTS)], back_recv.at[0])
     turned = (((0,), (0,)), ((), ()))
     out[...] = (
         lax.dot_general(weigh[0], returned[...], turned, preferred_element_type=jnp.float32)
@@ -576,8 +560,7 @@
     ).astype(jnp.bfloat16)
 
     loads[4].wait()
-    for offset in range(1, 8):
-        landed(gathered.at[(t + offset) % 8], at_recv.at[offset])
+    landed(gathered.at[pl.ds(0, 7)], at_recv.at[0])
     rows = jnp.concatenate([gathered[source] for source in range(8)], axis=1).astype(jnp.float32)
     inverse = lax.rsqrt(jnp.mean(rows * rows, axis=1, keepdims=True) + epsilon)
     normed = (rows * inverse * heads_gain[...]).astype(jnp.bfloat16)
@@ -585,14 +568,13 @@
         jnp.bfloat16
     )
 
-    for shape, sem in started:
-        if shape[-1] == PART:
-            room = partial.at[0, 0] if len(shape) == 3 else returned.at[pl.ds(0, shape[0])]
-        elif len(shape) == 3:
-            room = keys.at[pl.ds(0, 4), pl.ds(0, shape[1])]
-        else:
-            room = keys.at[0, pl.ds(0, shape[0])]
-        landed(room, sem[0].at[sem[1]])
+    rest = pl.ds(0, ALL_SLOTS - SLOTS)
+    landed(outgoing.at[rest], sent.at[0])
+    landed(features.at[pl.ds(0, 7)], sent.at[1])
+    landed(features.at[pl.ds(0, 7)], sent.at[2])
+    landed(result.at[rest], sent.at[3])
+    landed(keys.at[pl.ds(0, EXPERTS - 1)], sent.at[4])
+    landed(gathered.at[pl.ds(0, 7)], sent.at[5])
 
 
 def body(
@@ -644,24 +626,16 @@
             pltpu.VMEM((ROWS, 2 * HEAD), half),
             pltpu.VMEM((8, SHARE, 2 * HEAD), half),
             dma((5,)),
-            dma((EXPERTS,)),
-            dma((EXPERTS,)),
-            dma((CHUNKS, 8)),
-            dma((CHUNKS, 8)),
-            dma((CHUNKS, 5)),
-            dma((CHUNKS, 5)),
-            dma((EXPERTS,)),
-            dma((EXPERTS,)),
+            dma((6,)),
+            dma((CHUNKS,)),
+            dma((CHUNKS, 4)),
+            dma((CHUNKS, 4)),
+            dma((1,)),
             dma((2, 4)),
+            dma((PLANES, 3)),
+            dma((3,)),
             dma((2, 4)),
-            dma((PLANES, 4)),
-            dma((PLANES, 4)),
-            dma((4,)),
-            dma((4,)),
-            dma((2, 4)),
-            dma((2, 4)),
-            dma((8,)),
-            dma((8,)),
+            dma((1,)),
         ],
         compiler_params=pltpu.CompilerParams(
             collective_id=0, has_side_effects=True, vmem_limit_bytes=60 * 2**20

time: 86.5 us -> 81.1 us (0.938)
  the two profiles are of different devices: /device:TPU:225 before, /device:TPU:2 now
where the time goes in v4:
time: 81.1 us; the launch traced here: 80 us
  Pallas kernels  76.2 us (94%)
  local copies, waits for them, and re-layouts  3.14 us (4%)
    pallas_call x1, Pallas kernels, body(): pl.pallas_call(kernel, out_shape=(jax.ShapeDtypeStruct((TOKENS, PART), ha...  76.2 us
    unnamed x2, local copies, waits for them, and re-layouts  3.14 us

profile of v4, /device:TPU:2, one launch (start us, length us, event | category | flops | bytes accessed | tf_op | source)
XLA Modules:
  0.0 80.0 jit_solution(13461208014897254602)
XLA Ops:
  0.6 76.2 %shard_map.131 = (bf16[128,256]{1,0:T(8,128)(2,1)}, bf16[64,2048]{1,0:T(8,128)(2,1)}) custom-call(bf16[128,2048]{1,0:T(8,128)(2,1)} %tokens.1, f32[1,2048]{1,0:T(1,128)} %bitcast.10, s32[4,128]{1,0:T(4,128)} %bitcast.12, f32[4,128]{1,0:T(4,128)} %bitcast.13, bf16[2048,256]{1,0:T(8,128)(2,1)} %bitcast.7, bf16[2048,256]{1,0:T(8,128)(2,1)} %bitcast.8, ...), custom_call_target="tpu_custom_call" | custom-call | tf_op jit(solution)/shard_map/pallas_call | solution.py:598
  76.8 1.7 %copy.16 = bf16[64,2048]{1,0:T(8,128)(2,1)} copy(bf16[64,2048]{1,0:T(8,128)(2,1)} %get-tuple-element.8) | data formatting | bytes 524288
  78.5 1.5 %copy.17 = bf16[128,256]{1,0:T(8,128)(2,1)} copy(bf16[128,256]{1,0:T(8,128)(2,1)} %get-tuple-element.9) | data formatting | bytes 131072

commit v5 on v4

--- a/solution.py
+++ b/solution.py
@@ -552,13 +552,6 @@
         )
     gathered[t] = attended[pl.ds(pl.multiple_of(t * SHARE, SHARE), SHARE), :]
 
-    landed(returned.at[pl.ds(SLOTS, ALL_SLOTS - SLOTS)], back_recv.at[0])
-    turned = (((0,), (0,)), ((), ()))
-    out[...] = (
-        lax.dot_general(weigh[0], returned[...], turned, preferred_element_type=jnp.float32)
-        + lax.dot_general(weigh[1], returned[...], turned, preferred_element_type=jnp.float32)
-    ).astype(jnp.bfloat16)
-
     loads[4].wait()
     landed(gathered.at[pl.ds(0, 7)], at_recv.at[0])
     rows = jnp.concatenate([gathered[source] for source in range(8)], axis=1).astype(jnp.float32)
@@ -567,6 +560,13 @@
     mixer_out[...] = jnp.dot(normed, mix[...], preferred_element_type=jnp.float32).astype(
         jnp.bfloat16
     )
+
+    landed(returned.at[pl.ds(SLOTS, ALL_SLOTS - SLOTS)], back_recv.at[0])
+    turned = (((0,), (0,)), ((), ()))
+    out[...] = (
+        lax.dot_general(weigh[0], returned[...], turned, preferred_element_type=jnp.float32)
+        + lax.dot_general(weigh[1], returned[...], turned, preferred_element_type=jnp.float32)
+    ).astype(jnp.bfloat16)
 
     rest = pl.ds(0, ALL_SLOTS - SLOTS)
     landed(outgoing.at[rest], sent.at[0])

time: 81.1 us -> 80.1 us (0.988)
  Pallas kernels: 76.2 us -> 75.2 us
    pallas_call x1, Pallas kernels: 76.2 us -> 75.2 us  [body(): pl.pallas_call(kernel, out_shape=(jax.ShapeDtypeStruct((TOKENS, PART), ha...]
where the time goes in v5:
time: 80.1 us; the launch traced here: 79 us
  Pallas kernels  75.2 us (94%)
  local copies, waits for them, and re-layouts  3.14 us (4%)
    pallas_call x1, Pallas kernels, body(): pl.pallas_call(kernel, out_shape=(jax.ShapeDtypeStruct((TOKENS, PART), ha...  75.2 us
    unnamed x2, local copies, waits for them, and re-layouts  3.14 us

profile of v5, /device:TPU:2, one launch (start us, length us, event | category | flops | bytes accessed | tf_op | source)
XLA Modules:
  0.0 79.0 jit_solution(6345480665214020314)
XLA Ops:
  0.6 75.2 %shard_map.131 = (bf16[128,256]{1,0:T(8,128)(2,1)}, bf16[64,2048]{1,0:T(8,128)(2,1)}) custom-call(bf16[128,2048]{1,0:T(8,128)(2,1)} %tokens.1, f32[1,2048]{1,0:T(1,128)} %bitcast.10, s32[4,128]{1,0:T(4,128)} %bitcast.12, f32[4,128]{1,0:T(4,128)} %bitcast.13, bf16[2048,256]{1,0:T(8,128)(2,1)} %bitcast.7, bf16[2048,256]{1,0:T(8,128)(2,1)} %bitcast.8, ...), custom_call_target="tpu_custom_call" | custom-call | tf_op jit(solution)/shard_map/pallas_call | solution.py:598
  75.8 1.7 %copy.16 = bf16[64,2048]{1,0:T(8,128)(2,1)} copy(bf16[64,2048]{1,0:T(8,128)(2,1)} %get-tuple-element.8) | data formatting | bytes 524288
  77.5 1.5 %copy.17 = bf16[128,256]{1,0:T(8,128)(2,1)} copy(bf16[128,256]{1,0:T(8,128)(2,1)} %get-tuple-element.9) | data formatting | bytes 131072
